TPU v7x, 512 devices: a whole 4x4x16 slice. The times are simulated.
512 devices in a mesh: sp: 32 (over z, core), tp: 16 (over y, x).
Axes of the slice: x: 4, y: 4, z: 16, core: 2. Of those that a mesh axis runs over, the one named last changes fastest.
Arguments:
- moe_input: bfloat16 [4096, 2048], P('sp', 'tp'), may hold values from -6 to 6
- cotangent: bfloat16 [4096, 2048], P('sp', 'tp'), may hold values from -6 to 6
- routes: int32 [4096, 2], P('sp'), may hold values from 0 to 31, all different within a row; in each aligned block of 128 rows (0 to 127, 128 to 255, ...) at most 10 rows name the same one
- route_weights: float32 [4096, 2], P('sp'), may hold values from 0.2 to 1
- gate_branch: bfloat16 [4096, 2560], P('sp', 'tp'), may hold values from -6 to 6
- log_decay: float32 [4096, 2560], P('sp', 'tp'), may hold values from -0.12 to 0
- states: float32 [4096, 2560], P('sp', 'tp'), may hold values from -6 to 6
- w_gate: bfloat16 [32, 2048, 2048], P('sp', None, 'tp'), may hold values from -0.125 to 0.125
- w_up: bfloat16 [32, 2048, 2048], P('sp', None, 'tp'), may hold values from -0.125 to 0.125
- w_down: bfloat16 [32, 2048, 2048], P('sp', 'tp'), may hold values from -0.125 to 0.125
- out_proj: bfloat16 [2048, 2560], P('sp', 'tp'), may hold values from -0.125 to 0.125
Outputs:
- grad_w_gate: float32 [32, 2048, 2048], P('sp', None, 'tp')
- grad_w_up: float32 [32, 2048, 2048], P('sp', None, 'tp')
- grad_w_down: float32 [32, 2048, 2048], P('sp', 'tp')
- grad_out_proj: float32 [2048, 2560], P('sp', 'tp')
- grad_gate_branch: bfloat16 [4096, 2560], P('sp', 'tp')
- grad_log_decay: bfloat16 [4096, 2560], P('sp', 'tp')
- grad_input_term: float32 [4096, 2560], P('sp', 'tp')
Inputs may be any that keep to these rules, and one draw needn't show every extreme that they name: `routes`: in the rows of one device no expert is named by more than 10 entries, and in every draw some expert is named by exactly 10 entries of one device's rows.
All inputs are finite; a program needn't handle non-finite values.
Results may differ from a plain program's by a relative error of at most 0.025.
Values may be sent and summed in bfloat16 or wider, within the bound.
A program may use at most 64 MiB of HBM per device.

v0:
```python
import functools

import jax
import jax.numpy as jnp
from jax import lax
from jax.experimental import pallas as pl
from jax.experimental.pallas import tpu as pltpu
from jax.sharding import Mesh
from jax.sharding import PartitionSpec as P

BF = jnp.bfloat16
F32 = jnp.float32
I32 = jnp.int32
MESH = pl.DeviceIdType.MESH
LANES = 128
NZ = 16
CAP = 10
MSG = 24
RET = 16
ROWS = 2 * NZ * CAP
CHUNK = ROWS // 2
HALF = CHUNK // 2


def place(step):
    return max(2 * step - 1, 0) if step <= NZ // 2 else 2 * (NZ - step)


STEP_AT = [0] * NZ
for _step in range(NZ):
    STEP_AT[place(_step)] = _step


def dot(a, b):
    return jnp.dot(a, b, preferred_element_type=F32)


def dot_t(a, b):
    return lax.dot_general(a, b, (((1,), (1,)), ((), ())), preferred_element_type=F32)


def iota(shape, dim):
    return lax.broadcasted_iota(I32, shape, dim)


def landed(ref, sem):
    pltpu.make_async_copy(ref, ref, sem).wait()


class Spot:
    def __init__(self):
        self.sp = lax.axis_index("sp")
        self.tp = lax.axis_index("tp")
        self.z, self.c = self.sp // 2, self.sp % 2
        self.y, self.x = self.tp // 4, self.tp % 4

    def col(self, axis, by):
        return lax.rem(getattr(self, axis) + (by + 4), 4)

    def tpi(self, axis, by, other=0):
        a = self.col(axis, by)
        if axis == "x":
            return self.col("y", other) * 4 + a
        return a * 4 + self.col("x", other)

    def peer(self, axis, by):
        return (self.sp, self.tpi(axis, by))


def send(src, dst, ssem, rsem, dev, log):
    cp = pltpu.make_async_remote_copy(
        src_ref=src, dst_ref=dst, send_sem=ssem, recv_sem=rsem, device_id=dev, device_id_type=MESH
    )
    cp.start()
    log.append(cp)


class PlaneGather:
    def __init__(self, spot, buf, r0, n, u, ssem, rsem, log):
        self.s, self.buf, self.r0, self.n, self.u = spot, buf, r0, n, u
        self.v = "y" if u == "x" else "x"
        self.ssem, self.rsem, self.log = ssem, rsem, log
        self.sent = 0
        self.fu = (0, -1, 1, 2)

    def view(self, du, dv, half=None):
        r0, n = self.r0, self.n
        if half is not None:
            n = n // 2
            r0 = r0 + half * n
        lane = pl.multiple_of(self.s.tpi(self.u, du, dv) * LANES, LANES)
        return self.buf.at[pl.ds(r0, n), pl.ds(lane, LANES)]

    def go(self, view, axis, by, k):
        send(view, view, self.ssem.at[self.sent], self.rsem.at[k], self.s.peer(axis, by), self.log)
        self.sent += 1

    def fan(self, j):
        view = self.view(self.fu[j], 0)
        self.go(view, self.v, 1, 4 + 4 * j)
        self.go(view, self.v, -1, 5 + 4 * j)

    def stage0(self):
        view = self.view(0, 0)
        self.go(view, self.u, 1, 0)
        self.go(view, self.u, -1, 1)
        self.fan(0)

    def stage1(self):
        landed(self.view(-1, 0), self.rsem.at[0])
        self.go(self.view(-1, 0, 0), self.u, 1, 2)
        self.fan(1)
        landed(self.view(1, 0), self.rsem.at[1])
        self.go(self.view(1, 0, 1), self.u, -1, 3)
        self.fan(2)

    def relay(self, j):
        du = self.fu[j]
        landed(self.view(du, -1), self.rsem.at[4 + 4 * j])
        self.go(self.view(du, -1, 0), self.v, 1, 6 + 4 * j)
        landed(self.view(du, 1), self.rsem.at[5 + 4 * j])
        self.go(self.view(du, 1, 1), self.v, -1, 7 + 4 * j)

    def stage2(self):
        self.relay(0)

    def stage3(self):
        landed(self.view(2, 0, 0), self.rsem.at[2])
        landed(self.view(2, 0, 1), self.rsem.at[3])
        self.fan(3)

    def stage4(self):
        self.relay(1)
        self.relay(2)

    def stage5(self):
        self.relay(3)

    def stage6(self):
        for j in range(4):
            landed(self.view(self.fu[j], 2, 0), self.rsem.at[6 + 4 * j])
            landed(self.view(self.fu[j], 2, 1), self.rsem.at[7 + 4 * j])


def run_gathers(gathers):
    for k in range(7):
        for g in gathers:
            getattr(g, f"stage{k}")()


class PlaneSum:
    def __init__(self, spot, buf, r0, u, one_l, one_r, two_l, two_r, part, a_l, a_r, b_l, b_r, tmp, ssem, rsem, log):
        self.s, self.buf, self.r0, self.u = spot, buf, r0, u
        self.v = "y" if u == "x" else "x"
        self.one = (one_l, one_r)
        self.two = (two_l, two_r)
        self.part, self.a, self.b, self.tmp = part, (a_l, a_r), (b_l, b_r), tmp
        self.ssem, self.rsem, self.log = ssem, rsem, log

    def block(self, du, r0, n):
        a = self.s.col(self.u, du)
        if self.u == "x":
            return self.buf.at[:, a, pl.ds(r0, n), :]
        return self.buf.at[a, :, pl.ds(r0, n), :]

    def go(self, src, dst, axis, by, k):
        send(src, dst, self.ssem.at[k], self.rsem.at[k], self.s.peer(axis, by), self.log)

    def stage0(self):
        self.go(self.block(2, self.r0, HALF), self.one[0], self.u, 1, 0)
        self.go(self.block(2, self.r0 + HALF, HALF), self.one[1], self.u, -1, 1)

    def stage1(self):
        for side, by in ((0, 1), (1, -1)):
            landed(self.one[side], self.rsem.at[side])
            mine = self.block(by, self.r0 + side * HALF, HALF)
            mine[...] = (mine[...].astype(F32) + self.one[side][...].astype(F32)).astype(BF)
            self.go(self.block(by, self.r0, CHUNK), self.two[side], self.u, by, 2 + side)

    def stage2(self):
        landed(self.two[0], self.rsem.at[2])
        landed(self.two[1], self.rsem.at[3])
        own = self.block(0, self.r0, CHUNK)
        self.part[...] = (
            own[...].astype(F32) + self.two[0][...].astype(F32) + self.two[1][...].astype(F32)
        ).astype(BF)
        far = self.s.col(self.v, 2)
        self.go(self.part.at[far, pl.ds(0, HALF), :], self.a[0], self.v, 1, 4)
        self.go(self.part.at[far, pl.ds(HALF, HALF), :], self.a[1], self.v, -1, 5)

    def stage3(self):
        for side, by in ((0, 1), (1, -1)):
            landed(self.a[side], self.rsem.at[4 + side])
            near = self.s.col(self.v, by)
            mine = self.part.at[near, pl.ds(side * HALF, HALF), :]
            mine[...] = (mine[...].astype(F32) + self.a[side][...].astype(F32)).astype(BF)
            self.go(self.part.at[near], self.b[side], self.v, by, 6 + side)

    def stage4(self):
        landed(self.b[0], self.rsem.at[6])
        landed(self.b[1], self.rsem.at[7])
        own = self.part[self.s.col(self.v, 0)]
        total = own.astype(F32) + self.b[0][...].astype(F32) + self.b[1][...].astype(F32)
        return total.astype(BF)


def dest(spot, step, core):
    return (2 * lax.rem(spot.z + (NZ - step), NZ) + core, spot.tp)


def origin(spot, step, core):
    return (2 * lax.rem(spot.z + step, NZ) + core, spot.tp)


def group_of(expert, z):
    step = lax.rem(z - expert // 2 + NZ, NZ)
    at = jnp.where(step <= NZ // 2, jnp.maximum(2 * step - 1, 0), 2 * (NZ - step))
    return at * 2 + expert % 2


def slots_by_lane(routes_t, z):
    tok = routes_t.shape[1]
    hot = [(iota((32, tok), 0) == routes_t[k : k + 1, :]) for k in range(2)]
    both = (hot[0] | hot[1]).astype(F32).astype(BF)
    earlier = (iota((tok, tok), 0) < iota((tok, tok), 1)).astype(F32).astype(BF)
    before = dot(both, earlier)
    slot = [jnp.sum(jnp.where(h, before, 0.0), axis=0, keepdims=True).astype(I32) for h in hot]
    return [(group_of(routes_t[k : k + 1, :], z), slot[k]) for k in range(2)]


def slots_by_row(routes, z):
    tok = routes.shape[0]
    hot = [(iota((tok, 32), 1) == routes[:, k : k + 1]) for k in range(2)]
    both = (hot[0] | hot[1]).astype(F32).astype(BF)
    earlier = (iota((tok, tok), 1) < iota((tok, tok), 0)).astype(F32).astype(BF)
    before = dot(earlier, both)
    slot = [jnp.sum(jnp.where(h, before, 0.0), axis=1, keepdims=True).astype(I32) for h in hot]
    return [(group_of(routes[:, k : k + 1], z), slot[k]) for k in range(2)]


def k1_body(
    x_ref, cot_ref, routes_ref, routes_t_ref, rw_ref, wg_ref, wu_ref, wd_ref,
    rows_out, scaled_out, gp_out, hidden_out, tok_out,
    msg, arrived, xr, cr, wcat, wdv, gp, hid, terms, ret, back,
    a1l, a1r, a2l, a2r, apart, aal, aar, abl, abr,
    b1l, b1r, b2l, b2r, bpart, bal, bar, bbl, bbr,
    wsem, osem, d_s, d_r, g_s, g_r, q_s, q_r, r_s, r_r,
):
    s = Spot()
    log = []
    barrier = pltpu.get_barrier_semaphore()
    peers = 0
    for step in range(NZ):
        for core in range(2):
            if step == 0 and core == 0:
                dev = (2 * s.z + (1 - s.c), s.tp)
            elif step == 0:
                continue
            else:
                dev = dest(s, step, core)
            pl.semaphore_signal(barrier, inc=1, device_id=dev, device_id_type=MESH)
            peers += 1
    for axis in ("x", "y"):
        for by in (1, -1):
            pl.semaphore_signal(barrier, inc=1, device_id=s.peer(axis, by), device_id_type=MESH)
            peers += 1

    loads = [
        pltpu.make_async_copy(wg_ref.at[0], wcat.at[:, pl.ds(0, LANES)], wsem.at[0]),
        pltpu.make_async_copy(wu_ref.at[0], wcat.at[:, pl.ds(LANES, LANES)], wsem.at[1]),
        pltpu.make_async_copy(wd_ref.at[0], wdv, wsem.at[2]),
    ]
    for cp in loads:
        cp.start()

    by_lane = slots_by_lane(routes_t_ref[...], s.z)
    rows = [g * MSG + t for g, t in by_lane]
    at = iota((32 * MSG, LANES), 0)
    cot32 = cot_ref[...].astype(F32)
    picks = jnp.concatenate(
        [
            ((at == rows[0]) | (at == rows[1])).astype(F32).astype(BF),
            (at == rows[0] + CAP).astype(F32).astype(BF),
            (at == rows[1] + CAP).astype(F32).astype(BF),
        ],
        axis=1,
    )
    stuff = jnp.concatenate(
        [x_ref[...]] + [(rw_ref[:, k : k + 1] * cot32).astype(BF) for k in range(2)], axis=0
    )
    packed = dot(picks, stuff)
    for g in range(32):
        msg[g] = packed[g * MSG : (g + 1) * MSG, :].astype(BF)

    pl.semaphore_wait(barrier, peers)

    for chunk in range(2):
        for pos in range(chunk * 8, chunk * 8 + 8):
            step = STEP_AT[pos]
            for core in range(2):
                if step == 0:
                    if core == 1:
                        continue
                    src, dev = msg.at[1 - s.c], (2 * s.z + (1 - s.c), s.tp)
                    k = 0
                else:
                    k = 2 * pos + core
                    src, dev = msg.at[k], dest(s, step, core)
                send(src, arrived.at[2 * pos + s.c], d_s.at[k], d_r.at[chunk], dev, log)
    arrived[pl.ds(s.c, 1)] = msg[pl.ds(s.c, 1)]

    ri = iota((2 * CHUNK, 16 * MSG), 0)
    ci = iota((2 * CHUNK, 16 * MSG), 1)
    second = ri >= CHUNK
    rr = jnp.where(second, ri - CHUNK, ri)
    squeeze = (ci == (rr // CAP) * MSG + rr % CAP + jnp.where(second, CAP, 0)).astype(F32).astype(BF)

    own = pl.ds(pl.multiple_of(s.tp * LANES, LANES), LANES)
    gathers = []
    for chunk in range(2):
        waited = arrived.at[pl.ds(0, 15)] if chunk == 0 else arrived.at[pl.ds(16, 16)]
        landed(waited, d_r.at[chunk])
        block = jnp.concatenate(
            [arrived[16 * chunk + i].astype(F32) for i in range(16)], axis=0
        ).astype(BF)
        tight = dot(squeeze, block).astype(BF)
        span = pl.ds(chunk * CHUNK, CHUNK)
        xr[span, own] = tight[:CHUNK]
        cr[span, own] = tight[CHUNK:]
        pair = [
            PlaneGather(s, xr, chunk * CHUNK, CHUNK, "x", g_s.at[2 * chunk], g_r.at[2 * chunk], log),
            PlaneGather(s, cr, chunk * CHUNK, CHUNK, "y", g_s.at[2 * chunk + 1], g_r.at[2 * chunk + 1], log),
        ]
        for g in pair:
            g.stage0()
        gathers.append(pair)
    for pair in gathers:
        for k in range(1, 7):
            for g in pair:
                getattr(g, f"stage{k}")()
    for cp in loads:
        cp.wait()

    saves = [
        pltpu.make_async_copy(xr, rows_out, osem.at[0]),
        pltpu.make_async_copy(cr, scaled_out, osem.at[1]),
    ]
    for cp in saves:
        cp.start()

    sums = [
        PlaneSum(s, terms, 0, "x", a1l, a1r, a2l, a2r, apart, aal, aar, abl, abr, None, q_s.at[0], q_r.at[0], log),
        PlaneSum(s, terms, CHUNK, "y", b1l, b1r, b2l, b2r, bpart, bal, bar, bbl, bbr, None, q_s.at[1], q_r.at[1], log),
    ]
    for chunk in range(2):
        span = pl.ds(chunk * CHUNK, CHUNK)
        pre = dot(xr[span, :], wcat[...])
        gate, up = pre[:, :LANES], pre[:, LANES:]
        sig = jax.nn.sigmoid(gate)
        act = gate * sig
        slope = sig * (1.0 + gate * (1.0 - sig))
        hid[span, :] = (act * up).astype(BF)
        gh = dot_t(cr[span, :], wdv[...])
        both = jnp.concatenate([(gh * up * slope).astype(BF), (gh * act).astype(BF)], axis=1)
        gp[span, :] = both
        for far in (2, 1, 3, 0):
            for i in range(2):
                places = []
                for k in (2 * i, 2 * i + 1):
                    if chunk == 0:
                        places.append((k, s.col("x", far)))
                    else:
                        places.append((s.col("y", far), k))
                w2 = jnp.concatenate(
                    [wcat[pl.ds(pl.multiple_of((a * 4 + b) * LANES, LANES), LANES), :] for a, b in places],
                    axis=0,
                )
                t2 = dot_t(both, w2).astype(BF)
                for n, (a, b) in enumerate(places):
                    terms[a, b, span, :] = t2[:, n * LANES : (n + 1) * LANES]
            if far == 2:
                sums[chunk].stage0()
    saves += [
        pltpu.make_async_copy(gp, gp_out, osem.at[2]),
        pltpu.make_async_copy(hid, hidden_out, osem.at[3]),
    ]
    for cp in saves[2:]:
        cp.start()
    for k in range(1, 4):
        for q in sums:
            getattr(q, f"stage{k}")()

    ri = iota((16 * RET, CHUNK), 0)
    ci = iota((16 * RET, CHUNK), 1)
    spread = ((ri % RET < CAP) & (ci == (ri // RET) * CAP + ri % RET)).astype(F32).astype(BF)
    for chunk in range(2):
        total = sums[chunk].stage4()
        ret[pl.ds(16 * chunk, 16)] = dot(spread, total).astype(BF).reshape(16, RET, LANES)
        for pos in range(chunk * 8, chunk * 8 + 8):
            step = STEP_AT[pos]
            for core in range(2):
                if step == 0:
                    if core == 1:
                        continue
                    src, dev = ret.at[1 - s.c], (2 * s.z + (1 - s.c), s.tp)
                    k = 0
                else:
                    k = 2 * pos + core
                    src, dev = ret.at[k], origin(s, step, core)
                send(src, back.at[2 * pos + s.c], r_s.at[k], r_r.at[chunk], dev, log)
    back[pl.ds(s.c, 1)] = ret[pl.ds(s.c, 1)]
    by_row = slots_by_row(routes_ref[...], s.z)
    lane = iota((LANES, 32 * RET), 1)
    want = ((lane == by_row[0][0] * RET + by_row[0][1]) | (lane == by_row[1][0] * RET + by_row[1][1]))
    want = want.astype(F32).astype(BF)
    landed(back.at[pl.ds(0, 15)], r_r.at[0])
    landed(back.at[pl.ds(16, 16)], r_r.at[1])
    sums_back = dot(want, back[...].reshape(32 * RET, LANES))
    tok_out[...] = (cot32 + sums_back).astype(BF)
    for cp in log:
        cp.wait_send()
    for cp in saves:
        cp.wait()


def k1(x, cot, routes, routes_t, rw, wg, wu, wd):
    vm = pl.BlockSpec(memory_space=pltpu.VMEM)
    hb = pl.BlockSpec(memory_space=pl.ANY)
    d = 16 * LANES
    V = pltpu.VMEM
    dma = pltpu.SemaphoreType.DMA
    sums = lambda: [
        V((4, HALF, LANES), BF), V((4, HALF, LANES), BF), V((4, CHUNK, LANES), BF), V((4, CHUNK, LANES), BF),
        V((4, CHUNK, LANES), BF),
        V((HALF, LANES), BF), V((HALF, LANES), BF), V((CHUNK, LANES), BF), V((CHUNK, LANES), BF),
    ]
    return pl.pallas_call(
        k1_body,
        out_shape=[
            jax.ShapeDtypeStruct((ROWS, d), BF), jax.ShapeDtypeStruct((ROWS, d), BF),
            jax.ShapeDtypeStruct((ROWS, 2 * LANES), BF), jax.ShapeDtypeStruct((ROWS, LANES), BF),
            jax.ShapeDtypeStruct((LANES, LANES), BF),
        ],
        in_specs=[vm] * 5 + [hb] * 3,
        out_specs=[hb] * 4 + [vm],
        scratch_shapes=[
            V((32, MSG, LANES), BF), V((32, MSG, LANES), BF), V((ROWS, d), BF), V((ROWS, d), BF),
            V((d, 2 * LANES), BF), V((LANES, d), BF), V((ROWS, 2 * LANES), BF), V((ROWS, LANES), BF),
            V((4, 4, ROWS, LANES), BF), V((32, RET, LANES), BF), V((32, RET, LANES), BF),
            *sums(), *sums(),
            dma((3,)), dma((4,)), dma((32,)), dma((2,)), dma((4, 20)), dma((4, 20)),
            dma((2, 8)), dma((2, 8)), dma((32,)), dma((2,)),
        ],
        compiler_params=pltpu.CompilerParams(
            collective_id=0, has_side_effects=True, vmem_limit_bytes=56 * 1024 * 1024
        ),
        name="routed",
    )(x, cot, routes, routes_t, rw, wg, wu, wd)


SP = ("sp_0", "sp_1")


def in_one_piece(arrays, axis, split_dim, concat_dim, along):
    both = jnp.concatenate(arrays, axis=along)
    out, at, gathered = (
        lax.all_to_all(both, axis, split_axis=split_dim, concat_axis=concat_dim, tiled=True),
        0,
        [],
    )
    for a in arrays:
        gathered.append(lax.slice_in_dim(out, at, at + a.shape[along], axis=along))
        at += a.shape[along]
    return tuple(gathered)


def in_one_piece_2(arrays, axis, dim, along):
    both = jnp.concatenate(arrays, axis=along)
    out, at, gathered = (lax.all_gather(both, axis, axis=dim, tiled=True), 0, [])
    for a in arrays:
        gathered.append(lax.slice_in_dim(out, at, at + a.shape[along], axis=along))
        at += a.shape[along]
    return tuple(gathered)


def in_blocks(shard, dim, size):
    shape = shard.shape
    tiles = shard.reshape(*shape[:dim], size, shape[dim] // size, *shape[dim + 1 :])
    return jnp.moveaxis(tiles, dim, 0)


def sent_and_summed(shard, axis, dim):
    size = lax.axis_size(axis)
    tiles = lax.all_to_all(in_blocks(shard, dim, size), axis, 0, 0, tiled=True)
    return jnp.sum(tiles.astype(jnp.float32), axis=0)


def in_order(tiles, dim):
    shape = list(tiles.shape[1:])
    shape[dim] *= tiles.shape[0]
    return jnp.moveaxis(tiles, 0, dim).reshape(shape)


def copy_for_each(shard, axis):
    size = lax.axis_size(axis)
    return lax.all_to_all(
        jnp.broadcast_to(shard[None], (size, *shard.shape)), axis, 0, 0, tiled=True
    )


def gathered_copies(shard, axis, dim):
    return in_order(copy_for_each(shard, axis), dim)


def own_block(tiles, axes, order):
    inside = tiles.shape[1:]
    tiles = tiles.reshape(*(lax.axis_size(a) for a in axes), *inside)
    tiles = jnp.moveaxis(tiles, order, range(len(axes))).reshape(-1, *inside)
    for k in order:
        tiles = lax.psum_scatter(tiles, axes[k], scatter_dimension=0, tiled=True)
    return tiles[0]


def summed_rows_2(shard, axes, order, dim):
    size = lax.axis_size(axes)
    return own_block(in_blocks(shard, dim, size), axes, order)


def all_blocks(shard, axes, order):
    tiles = shard[None]
    for k in order:
        tiles = lax.all_gather(tiles, axes[k], axis=0, tiled=True)
    current = [lax.axis_size(axes[k]) for k in reversed(order)]
    tiles = tiles.reshape(*current, *shard.shape)
    turned = sorted(range(len(order)), key=lambda place: order[len(order) - 1 - place])
    return tiles.transpose(*turned, *range(len(order), tiles.ndim)).reshape(-1, *shard.shape)


def gathered_by_axis(shard, axes, order, dim):
    return in_order(all_blocks(shard, axes, order), dim)


def all_in_one(shard, axis):
    leaves = jax.tree.leaves(shard)
    order = sorted(range(len(leaves)), key=lambda k: -leaves[k].size)
    width = (1, *leaves[order[0]].shape)[-1]
    lines = [
        jnp.pad(leaves[k].reshape(-1), (0, -leaves[k].size % width)).reshape(-1, width)
        for k in order
    ]
    both, at, found = (copy_for_each(jnp.concatenate(lines), axis), 0, {})
    for k, line in zip(order, lines):
        slab = both[:, at : at + len(line)].reshape(len(both), -1)
        found[k] = slab[:, : leaves[k].size].reshape(-1, *leaves[k].shape)
        at += len(line)
    numbers = iter(range(len(leaves)))
    return jax.tree.map(lambda _: found[next(numbers)], shard)


def joined_by_halves(pieces, combine):
    while len(jax.tree.leaves(pieces)[0]) > 1:
        pieces = jax.vmap(combine)(
            *(jax.tree.map(lambda part: part[side::2], pieces) for side in (0, 1))
        )
    return jax.tree.map(lambda part: part[0], pieces)


def carried_in(shard, axis, combine, identity):
    size, mine = (lax.axis_size(axis), lax.axis_index(axis))
    passed = jnp.arange(size) > mine

    def kept(part, zero, own):
        part = jnp.where(
            passed.reshape(-1, *(1 for _ in own.shape)), part, jnp.asarray(zero, own.dtype)
        )
        return part[::-1]

    pieces = all_in_one(shard, axis)
    return joined_by_halves(jax.tree.map(kept, pieces, identity, shard), combine)


def from_behind(value, axis, steps):
    count = lax.axis_size(axis)
    leading, last = (max(0, -steps), min(count, count - steps))
    return lax.ppermute(value, axis, [(source, source + steps) for source in range(leading, last)])


def silu_parts(pre_gate):
    sigmoid_val = jax.nn.sigmoid(pre_gate)
    return (pre_gate * sigmoid_val, sigmoid_val * (1.0 + pre_gate * (1.0 - sigmoid_val)))


def combine_pair(left_pair, right_pair):
    return (left_pair[0] * right_pair[0], right_pair[0] * left_pair[1] + right_pair[1])


def compose_maps(earlier, later_map):
    return (earlier[0] * later_map[0], later_map[1] + later_map[0] * earlier[1])


def contract_rows(left_mat, right_mat):
    return lax.dot_general(
        left_mat, right_mat, (((0,), (0,)), ((), ())), preferred_element_type=jnp.float32
    )


def contract_cols(left_mat, right_mat):
    return lax.dot_general(
        left_mat, right_mat, (((1,), (1,)), ((), ())), preferred_element_type=jnp.float32
    )


def rest_shards(grad_cols, gate_branch, log_decay, states, out_proj):
    grad_tokens = gathered_copies(grad_cols, "tp", 1)
    active_gate, pullback = jax.vjp(jax.nn.gelu, gate_branch.astype(jnp.float32))
    mixed_in = (active_gate * states).astype(jnp.bfloat16)
    piece_cols = grad_tokens
    grad_out_proj = summed_rows_2(
        contract_rows(piece_cols, mixed_in).astype(jnp.bfloat16), SP, (1, 0), 0
    ).astype(jnp.float32)
    piece_cols = grad_tokens
    grad_mixed = jnp.dot(
        piece_cols, gathered_by_axis(out_proj, SP, (0, 1), 0), preferred_element_type=jnp.float32
    )
    grad_gate_branch = pullback(grad_mixed * states)[0].astype(jnp.bfloat16)
    grad_state = grad_mixed * active_gate
    decays = jnp.exp(log_decay)
    next_decay = jnp.concatenate([decays[1:], jnp.ones_like(decays[:1])], axis=0)
    span_flip, local_flip = lax.associative_scan(
        combine_pair, (jnp.flip(next_decay, 0), jnp.flip(grad_state, 0))
    )
    span_decay = jnp.flip(span_flip, 0)
    local_grad = jnp.flip(local_flip, 0)
    whole_decay = span_decay[0] * decays[0]
    entry_term = decays[0] * local_grad[0]
    carried = carried_in(
        (whole_decay, entry_term),
        SP,
        compose_maps,
        (jnp.ones_like(whole_decay), jnp.zeros_like(entry_term)),
    )
    grad_input_term = local_grad + span_decay * carried[1][None, :]
    earlier_state = from_behind(states[-1:], SP, 1)
    prev_states = jnp.concatenate([earlier_state, states[:-1]], axis=0)
    grad_log_decay = (grad_input_term * decays * prev_states).astype(jnp.bfloat16)
    return grad_out_proj, grad_gate_branch, grad_log_decay, grad_input_term


def expert_shards(moe_input, cotangent, routes, route_weights, w_gate, w_up, w_down):
    rows, scaled, gp, hidden, tok = k1(
        moe_input, cotangent, routes, routes.T, route_weights, w_gate, w_up, w_down
    )
    half = gp.shape[1] // 2
    return (
        contract_rows(rows, gp[:, :half])[None],
        contract_rows(rows, gp[:, half:])[None],
        contract_rows(hidden, scaled)[None],
        tok,
    )


def solution(mesh):
    finer = Mesh(mesh.devices.reshape(16, 2, mesh.shape["tp"]), ("sp_0", "sp_1", "tp"))
    f1 = jax.shard_map(
        expert_shards,
        mesh=mesh,
        in_specs=(
            P("sp", "tp"), P("sp", "tp"), P("sp", None), P("sp", None),
            P("sp", None, "tp"), P("sp", None, "tp"), P("sp", "tp", None),
        ),
        out_specs=(P("sp", None, "tp"), P("sp", None, "tp"), P("sp", "tp", None), P("sp", "tp")),
        check_vma=False,
    )
    f2 = jax.shard_map(
        rest_shards, mesh=finer, in_specs=(P(SP, "tp"),) * 5, out_specs=(P(SP, "tp"),) * 4, check_vma=False
    )

    def whole(
        moe_input, cotangent, routes, route_weights, gate_branch, log_decay, states, w_gate, w_up, w_down, out_proj
    ):
        gg, gu, gd, tok = f1(moe_input, cotangent, routes, route_weights, w_gate, w_up, w_down)
        return (gg, gu, gd, *f2(tok, gate_branch, log_decay, states, out_proj))

    return whole
```

profile of v0, /device:TPU:2, one launch (start us, length us, event | category | flops | bytes accessed | tf_op | source)
XLA Modules:
  0.0 297.6 jit_solution(11761741751540929971)
XLA Ops:
  7.2 1.4 copy.75.routes_ref
  8.6 1.4 copy.76.rw_ref
  10.0 84.3 %routed.1 = (bf16[320,2048]{1,0:T(8,128)(2,1)}, bf16[320,2048]{1,0:T(8,128)(2,1)}, bf16[320,256]{1,0:T(8,128)(2,1)}, bf16[320,128]{1,0:T(8,128)(2,1)}, bf16[128,128]{1,0:T(8,128)(2,1)}) custom-call(bf16[128,128]{1,0:T(8,128)(2,1)} %x_ref.1, bf16[128,128]{1,0:T(8,128)(2,1)} %cot_ref.1, s32[128,2]{1,0:T(8,128)} %copy.75.routes_ref, s32[2,128]{1,0:T(2,128)} %bitcast.63, ...), custom_call_target="tpu_custom_call" | custom-call | tf_op jit(solution)/shard_map/routed/pallas_call | solution.py:437
  94.3 0.9 copy.77
  95.2 0.9 broadcast_in_dim.48
  96.1 7.1 %all-to-all-start = ((bf16[16,128,128]{1,2,0:T(8,128)(2,1)}), bf16[16,128,128]{1,2,0:T(8,128)(2,1)S(1)}, u32[]{:S(2)}, u32[]{:S(2)}) async-start(bf16[16,128,128]{1,2,0:T(8,128)(2,1)} %broadcast_in_dim.48), calls=%async_computation | async-start | bytes 1048576 | tf_op jit(solution)/shard_map/all_to_all | solution.py:506
  103.2 0.7 slice.423
  103.9 2.1 collective-permute-start
  106.0 31.0 %all-gather = bf16[1024,160]{1,0:T(8,128)(2,1)S(1)} all-gather(bf16[64,160]{1,0:T(8,128)(2,1)S(1)} %copy-done.8), channel_id=2, replica_groups=mesh['sp_0'=16,'sp_1'=2,'tp'=16] {'sp_0'}, dimensions={0}, use_global_device_ids=true | all-gather | bytes 348160 | tf_op jit(solution)/shard_map/all_gather | solution.py:532
  137.0 2.9 all_gather.7
  140.0 1.4 slice.329
  141.4 1.4 slice.336
  142.8 1.4 slice.327
  144.3 1.4 copy.80
  145.7 0.3 slice.330
  146.0 0.3 slice.337
  146.3 0.3 slice.328
  146.6 2.5 convolution_bitcast_fusion.1
  149.1 1.6 convolution_bitcast_fusion.2
  150.8 1.1 fusion.18
  151.9 1.4 slice.331
  153.3 1.4 slice.333
  154.7 0.3 slice.332
  155.0 0.5 slice.334
  155.5 0.7 slice.340
  156.3 0.8 slice.341
  157.0 0.8 slice.339
  157.8 0.7 slice.343
  158.6 0.4 slice.346
  158.9 0.4 slice.347
  159.4 0.4 slice.345
  159.8 0.4 slice.349
  162.4 0.8 fusion.29
  164.1 0.4 slice.344
  164.5 0.4 slice.377
  164.9 0.7 slice.338
  165.6 0.7 slice.379
  166.4 1.4 slice.381
  167.9 0.3 fusion
  168.2 1.0 pad_maximum_fusion
  171.9 0.4 pad.96
  172.2 0.4 pad.97
  172.7 0.4 pad.111
  173.2 0.4 pad.110
  173.7 1.0 pad.112
  174.7 0.7 pad.113
  175.5 1.4 pad.115
  177.0 0.7 pad.98
  177.7 0.7 pad.99
  178.5 1.4 pad.101
  179.9 0.3 slice.382
  180.3 1.4 pad.100
  181.8 1.4 pad.114
  183.5 0.7 broadcast_in_dim.51
  184.2 7.5 %all-to-all-start.1 = ((f32[32,2,160]{2,1,0:T(2,128)}), f32[32,2,160]{2,1,0:T(2,128)S(1)}, u32[]{:S(2)}, u32[]{:S(2)}) async-start(f32[32,2,160]{2,1,0:T(2,128)} %broadcast_in_dim.51), calls=%async_computation.3 | async-start | bytes 131072 | tf_op jit(solution)/shard_map/all_to_all | solution.py:506
  191.7 0.5 copy.78
  192.2 1.0 copy.79
  193.4 0.6 copy-done.2
  193.9 1.4 convolution_bitcast_fusion
  196.0 10.0 %all-to-all-done.1 = f32[32,2,160]{2,1,0:T(2,128)S(1)} async-done(((f32[32,2,160]{2,1,0:T(2,128)}), f32[32,2,160]{2,1,0:T(2,128)S(1)}, u32[]{:S(2)}, u32[]{:S(2)}) %all-to-all-start.1) | async-done | bytes 40992 | tf_op jit(solution)/shard_map/all_to_all | solution.py:506
  206.8 8.3 %reduce-scatter.3.cloned.1.call-done = bf16[16,64,160]{2,1,0:T(8,128)(2,1)} async-done(((bf16[32,64,160]{2,1,0:T(8,128)(2,1)}), bf16[16,64,160]{2,1,0:T(8,128)(2,1)}) %reduce-scatter.3.cloned.1.call-update) | async-done | bytes 327696 | tf_op jit(solution)/shard_map/reduce_scatter | solution.py:520
  215.2 1.6 fusion.15
  216.8 72.6 %reduce-scatter.5.cloned.1.call-done = bf16[1,64,160]{2,1,0:T(8,128)(2,1)} async-done(((bf16[16,64,160]{2,1,0:T(8,128)(2,1)}), bf16[1,64,160]{2,1,0:T(8,128)(2,1)}) %reduce-scatter.5.cloned.1.call-update) | async-done | bytes 20496 | tf_op jit(solution)/shard_map/reduce_scatter | solution.py:520
  289.4 1.4 bitcast_convert_fusion
  (124 shorter events, 8.0 us)
Async XLA Ops:
  10.0 93.2 %copy-start.1 = (f32[128,160]{0,1:T(8,128)S(1)}, f32[128,160]{0,1:T(8,128)}, u32[]{:S(2)}) copy-start(f32[128,160]{0,1:T(8,128)} %param.21) | copy-start | bytes 245764
  94.3 11.7 %copy-start.8 = (bf16[64,160]{1,0:T(8,128)(2,1)S(1)}, bf16[64,160]{1,0:T(8,128)(2,1)}, u32[]{:S(2)}) copy-start(bf16[64,160]{1,0:T(8,128)(2,1)} %param.22) | copy-start | bytes 61444
  96.1 54.7 %all-to-all-start = ((bf16[16,128,128]{1,2,0:T(8,128)(2,1)}), bf16[16,128,128]{1,2,0:T(8,128)(2,1)S(1)}, u32[]{:S(2)}, u32[]{:S(2)}) async-start(bf16[16,128,128]{1,2,0:T(8,128)(2,1)} %broadcast_in_dim.48), calls=%async_computation | async-start | bytes 1048576 | tf_op jit(solution)/shard_map/all_to_all | solution.py:506
  103.2 36.7 %copy-start.3 = (f32[128,160]{0,1:T(8,128)S(1)}, f32[128,160]{0,1:T(8,128)}, u32[]{:S(2)}) copy-start(f32[128,160]{0,1:T(8,128)} %param.20) | copy-start | bytes 245764
  103.9 111.2 %collective-permute-start = (f32[1,160]{0,1:T(8,128)}, f32[1,160]{0,1:T(8,128)}, u32[]{:S(2)}, u32[]{:S(2)}) collective-permute-start(f32[1,160]{0,1:T(8,128)} %slice.423), channel_id=1, source_target_pairs={{0,16},{16,32},{32,48},{48,64},{64,80},{80,96},{96,112},{112,128},... | collective-permute-start | bytes 1928 | tf_op jit(solution)/shard_map/ppermute | solution.py:585
  144.3 2.3 copy-start
  146.6 2.6 copy-start.4
  149.1 1.6 copy-start.5
  163.2 4.6 %copy-start.6 = (bf16[128,160]{0,1:T(8,128)(2,1)S(1)}, bf16[128,160]{0,1:T(8,128)(2,1)}, u32[]{:S(2)}) copy-start(bf16[128,160]{0,1:T(8,128)(2,1)} %param.19) | copy-start | bytes 122884
  184.2 21.9 %all-to-all-start.1 = ((f32[32,2,160]{2,1,0:T(2,128)}), f32[32,2,160]{2,1,0:T(2,128)S(1)}, u32[]{:S(2)}, u32[]{:S(2)}) async-start(f32[32,2,160]{2,1,0:T(2,128)} %broadcast_in_dim.51), calls=%async_computation.3 | async-start | bytes 131072 | tf_op jit(solution)/shard_map/all_to_all | solution.py:506
  191.7 23.4 %reduce-scatter.3.cloned.1.call-start = ((), (), s32[]{:S(2)}) async-start(), calls=%async_computation.4 | async-start | bytes 1572864 | tf_op jit(solution)/shard_map/reduce_scatter | solution.py:520
  192.2 1.7 copy-start.2
  192.2 1.7 copy-start.7
  193.3 96.1 %reduce-scatter.5.cloned.1.call-start = ((), (), s32[]{:S(2)}) async-start(), calls=%async_computation.5 | async-start | bytes 557056 | tf_op jit(solution)/shard_map/reduce_scatter | solution.py:520
Sparse Core Ops, SparseCore 0:
  195.3 19.7 reduce-scatter.2
  217.9 71.4 reduce-scatter.4
where the time goes:
time: 298 us
  waiting for transfers between devices  90.9 us (31%)
  Pallas kernels  84.3 us (28%)
  local copies, waits for them, and re-layouts  43.2 us (14%)
  blocking collectives  33.9 us (11%)
  starting transfers between devices  16.7 us (6%)
  between operations  15 us (5%)
  matrix products  7.06 us (2%)
  other arithmetic  6.56 us (2%)
    pallas_call x1, Pallas kernels, k1(): pl.pallas_call(k1_body, out_shape=[jax.ShapeDtypeStruct((ROWS, d), BF), j...  84.3 us
    reduce_scatter x2, waiting for transfers between devices, own_block(): tiles = lax.psum_scatter(tiles, axes[k], scatter_dimension=0, tiled=True)  80.8 us
    all_gather x2, blocking collectives, all_blocks(): tiles = lax.all_gather(tiles, axes[k], axis=0, tiled=True)  33.9 us
    slice x41, local copies, waits for them, and re-layouts, rest_shards(): lax.associative_scan(combine_pair, (jnp.flip(next_decay, 0), jnp.flip(gra...  20 us
    all_to_all x2, starting transfers between devices, copy_for_each(): lax.all_to_all(jnp.broadcast_to(shard[None], (size, *shard.shape)), axis,...  14.6 us
    pad x24, local copies, waits for them, and re-layouts, rest_shards(): lax.associative_scan(combine_pair, (jnp.flip(next_decay, 0), jnp.flip(gra...  12.1 us
    all_to_all x2, waiting for transfers between devices, copy_for_each(): lax.all_to_all(jnp.broadcast_to(shard[None], (size, *shard.shape)), axis,...  10.1 us
  transfers between devices with their start and end apart: 5, of which 3 were waited for; matrix products, arithmetic and copies ran while one was open for 17% of the time, Pallas kernels for 0%

commit v1 on v0

v1 whole, which is shorter than its diff:
```python
import functools

import jax
import jax.numpy as jnp
from jax import lax
from jax.experimental import pallas as pl
from jax.experimental.pallas import tpu as pltpu
from jax.sharding import PartitionSpec as P

BF = jnp.bfloat16
F32 = jnp.float32
I32 = jnp.int32
MESH = pl.DeviceIdType.MESH
LANES = 128
NZ = 16
CAP = 10
MSG = 24
RET = 16
ROWS = 2 * NZ * CAP
CHUNK = ROWS // 2
HALF = CHUNK // 2


def place(step):
    return max(2 * step - 1, 0) if step <= NZ // 2 else 2 * (NZ - step)


STEP_AT = [0] * NZ
for _step in range(NZ):
    STEP_AT[place(_step)] = _step


def dot(a, b):
    return jnp.dot(a, b, preferred_element_type=F32)


def dot_t(a, b):
    return lax.dot_general(a, b, (((1,), (1,)), ((), ())), preferred_element_type=F32)


def iota(shape, dim):
    return lax.broadcasted_iota(I32, shape, dim)


def landed(ref, sem):
    pltpu.make_async_copy(ref, ref, sem).wait()


class Spot:
    def __init__(self):
        self.sp = lax.axis_index("sp")
        self.tp = lax.axis_index("tp")
        self.z, self.c = self.sp // 2, self.sp % 2
        self.y, self.x = self.tp // 4, self.tp % 4

    def col(self, axis, by):
        return lax.rem(getattr(self, axis) + (by + 4), 4)

    def tpi(self, axis, by, other=0):
        a = self.col(axis, by)
        if axis == "x":
            return self.col("y", other) * 4 + a
        return a * 4 + self.col("x", other)

    def peer(self, axis, by):
        return (self.sp, self.tpi(axis, by))


def send(src, dst, ssem, rsem, dev, log):
    cp = pltpu.make_async_remote_copy(
        src_ref=src, dst_ref=dst, send_sem=ssem, recv_sem=rsem, device_id=dev, device_id_type=MESH
    )
    cp.start()
    log.append(cp)


class PlaneGather:
    def __init__(self, spot, view, u, ssem, rsem, log, total=None):
        self.s, self.block, self.u = spot, view, u
        self.v = "y" if u == "x" else "x"
        self.ssem, self.rsem, self.log, self.total = ssem, rsem, log, total
        self.sent = 0
        self.fu = (0, -1, 1, 2)

    def view(self, du, dv, half=None):
        return self.block(self.s.tpi(self.u, du, dv), half)

    def go(self, view, axis, by, k):
        ssem = self.ssem.at[self.sent] if self.total is None else self.ssem
        log = self.log if self.total is None else []
        send(view, view, ssem, self.rsem.at[k], self.s.peer(axis, by), log)
        self.sent += 1

    def fan(self, j):
        view = self.view(self.fu[j], 0)
        self.go(view, self.v, 1, 4 + 4 * j)
        self.go(view, self.v, -1, 5 + 4 * j)

    def stage0(self):
        view = self.view(0, 0)
        self.go(view, self.u, 1, 0)
        self.go(view, self.u, -1, 1)
        self.fan(0)

    def stage1(self):
        landed(self.view(-1, 0), self.rsem.at[0])
        self.go(self.view(-1, 0, 0), self.u, 1, 2)
        self.fan(1)
        landed(self.view(1, 0), self.rsem.at[1])
        self.go(self.view(1, 0, 1), self.u, -1, 3)
        self.fan(2)

    def relay(self, j):
        du = self.fu[j]
        landed(self.view(du, -1), self.rsem.at[4 + 4 * j])
        self.go(self.view(du, -1, 0), self.v, 1, 6 + 4 * j)
        landed(self.view(du, 1), self.rsem.at[5 + 4 * j])
        self.go(self.view(du, 1, 1), self.v, -1, 7 + 4 * j)

    def stage2(self):
        self.relay(0)

    def stage3(self):
        landed(self.view(2, 0, 0), self.rsem.at[2])
        landed(self.view(2, 0, 1), self.rsem.at[3])
        self.fan(3)

    def stage4(self):
        self.relay(1)
        self.relay(2)

    def stage5(self):
        self.relay(3)

    def stage6(self):
        for j in range(4):
            landed(self.view(self.fu[j], 2, 0), self.rsem.at[6 + 4 * j])
            landed(self.view(self.fu[j], 2, 1), self.rsem.at[7 + 4 * j])

    def drain(self):
        if self.total is not None:
            landed(self.total, self.ssem)


def lane_blocks(buf, r0, n):
    def view(tpi, half):
        lane = pl.ds(pl.multiple_of(tpi * LANES, LANES), LANES)
        if half is None:
            return buf.at[pl.ds(r0, n), lane]
        return buf.at[pl.ds(r0 + half * (n // 2), n // 2), lane]

    return view


def row_blocks(buf, i0, n):
    def view(tpi, half):
        if half is None:
            return buf.at[pl.ds(i0, n), tpi % 2, tpi // 2]
        return buf.at[pl.ds(i0 + half * (n // 2), n // 2), tpi % 2, tpi // 2]

    return view


class Ring:
    def __init__(self, spot, part, ssem, rsem, log):
        self.s, self.part, self.ssem, self.rsem, self.log = spot, part, ssem, rsem, log

    def at(self, by):
        return lax.rem(self.s.z + (by + NZ), NZ)

    def go(self, way, k):
        by = 1 if way == 0 else -1
        dev = (2 * self.at(by) + self.s.c, self.s.tp)
        for n, view in enumerate(self.part(self.at(-by * k))):
            send(view, view, self.ssem.at[way, n, k], self.rsem.at[way, n, k], dev, self.log)

    def start(self):
        self.go(0, 0)
        self.go(1, 0)

    def step(self, k):
        for way, by, last in ((0, 1, 8), (1, -1, 7)):
            if k < last:
                for n, view in enumerate(self.part(self.at(-by * (k + 1)))):
                    landed(view, self.rsem.at[way, n, k])
                if k + 1 < last:
                    self.go(way, k + 1)


class PlaneSum:
    def __init__(self, spot, buf, r0, u, one_l, one_r, two_l, two_r, part, a_l, a_r, b_l, b_r, tmp, ssem, rsem, log):
        self.s, self.buf, self.r0, self.u = spot, buf, r0, u
        self.v = "y" if u == "x" else "x"
        self.one = (one_l, one_r)
        self.two = (two_l, two_r)
        self.part, self.a, self.b, self.tmp = part, (a_l, a_r), (b_l, b_r), tmp
        self.ssem, self.rsem, self.log = ssem, rsem, log

    def block(self, du, r0, n):
        a = self.s.col(self.u, du)
        if self.u == "x":
            return self.buf.at[:, a, pl.ds(r0, n), :]
        return self.buf.at[a, :, pl.ds(r0, n), :]

    def go(self, src, dst, axis, by, k):
        send(src, dst, self.ssem.at[k], self.rsem.at[k], self.s.peer(axis, by), self.log)

    def stage0(self):
        self.go(self.block(2, self.r0, HALF), self.one[0], self.u, 1, 0)
        self.go(self.block(2, self.r0 + HALF, HALF), self.one[1], self.u, -1, 1)

    def stage1(self):
        for side, by in ((0, 1), (1, -1)):
            landed(self.one[side], self.rsem.at[side])
            mine = self.block(by, self.r0 + side * HALF, HALF)
            mine[...] = (mine[...].astype(F32) + self.one[side][...].astype(F32)).astype(BF)
            self.go(self.block(by, self.r0, CHUNK), self.two[side], self.u, by, 2 + side)

    def stage2(self):
        landed(self.two[0], self.rsem.at[2])
        landed(self.two[1], self.rsem.at[3])
        own = self.block(0, self.r0, CHUNK)
        self.part[...] = (
            own[...].astype(F32) + self.two[0][...].astype(F32) + self.two[1][...].astype(F32)
        ).astype(BF)
        far = self.s.col(self.v, 2)
        self.go(self.part.at[far, pl.ds(0, HALF), :], self.a[0], self.v, 1, 4)
        self.go(self.part.at[far, pl.ds(HALF, HALF), :], self.a[1], self.v, -1, 5)

    def stage3(self):
        for side, by in ((0, 1), (1, -1)):
            landed(self.a[side], self.rsem.at[4 + side])
            near = self.s.col(self.v, by)
            mine = self.part.at[near, pl.ds(side * HALF, HALF), :]
            mine[...] = (mine[...].astype(F32) + self.a[side][...].astype(F32)).astype(BF)
            self.go(self.part.at[near], self.b[side], self.v, by, 6 + side)

    def stage4(self):
        landed(self.b[0], self.rsem.at[6])
        landed(self.b[1], self.rsem.at[7])
        own = self.part[self.s.col(self.v, 0)]
        total = own.astype(F32) + self.b[0][...].astype(F32) + self.b[1][...].astype(F32)
        return total.astype(BF)


def dest(spot, step, core):
    return (2 * lax.rem(spot.z + (NZ - step), NZ) + core, spot.tp)


def origin(spot, step, core):
    return (2 * lax.rem(spot.z + step, NZ) + core, spot.tp)


def group_of(expert, z):
    step = lax.rem(z - expert // 2 + NZ, NZ)
    at = jnp.where(step <= NZ // 2, jnp.maximum(2 * step - 1, 0), 2 * (NZ - step))
    return at * 2 + expert % 2


def slots_by_lane(routes_t, z):
    tok = routes_t.shape[1]
    hot = [(iota((32, tok), 0) == routes_t[k : k + 1, :]) for k in range(2)]
    both = (hot[0] | hot[1]).astype(F32).astype(BF)
    earlier = (iota((tok, tok), 0) < iota((tok, tok), 1)).astype(F32).astype(BF)
    before = dot(both, earlier)
    slot = [jnp.sum(jnp.where(h, before, 0.0), axis=0, keepdims=True).astype(I32) for h in hot]
    return [(group_of(routes_t[k : k + 1, :], z), slot[k]) for k in range(2)]


def shifted_up(v, by, fill):
    n = v.shape[0]
    if by % 8 == 0:
        return jnp.concatenate([v[by:], jnp.full((by, v.shape[1]), fill, v.dtype)], axis=0)
    return jnp.where(iota(v.shape, 0) < n - by, pltpu.roll(v, n - by, 0), fill)


def turned(v):
    if v.shape[1] == LANES:
        low = jnp.concatenate([v[LANES:], jnp.zeros((2 * LANES - v.shape[0], LANES), F32)], axis=0)
        return jnp.concatenate([v[:LANES].T, low.T[:, : v.shape[0] - LANES]], axis=1)
    wide = jnp.concatenate([v[:, LANES:], jnp.zeros((v.shape[0], 2 * LANES - v.shape[1]), F32)], axis=1)
    return jnp.concatenate([v[:, :LANES].T, wide.T[: v.shape[1] - LANES]], axis=0)


def body(
    x_ref, cot_ref, routes_t_ref, rw_t_ref, gate_ref, ld_ref, st_ref, op_ref, wg_ref, wu_ref, wd_ref,
    rows_out, scaled_out, gp_out, hidden_out, gop_out, ggb_out, gld_out, git_out,
    msg, arrived, xr, cr, wcat, wdv, gp, hid, terms, ret, back,
    a1l, a1r, a2l, a2r, apart, aal, aar, abl, abr,
    b1l, b1r, b2l, b2r, bpart, bal, bar, bbl, bbr,
    opsib, mx, opt, spans, act_v, dact_v, dec_v, prev_v,
    toks, gt, ent, whole, lastrow, prevrow, gops, gopr,
    wsem, osem, d_s, d_r, g_s, g_r, q_s, q_r, r_s, r_r,
    o_s, o_r, ring_s, ring_r, t_s, t_r, u_s, u_r, x_s, x_r, e_s, e_r, w_s, w_r, l_s, l_r, h_s, h_r, z_s, z_r,
):
    s = Spot()
    log = []
    sibling = (2 * s.z + (1 - s.c), s.tp)
    barrier = pltpu.get_barrier_semaphore()
    peers = 1
    pl.semaphore_signal(barrier, inc=1, device_id=sibling, device_id_type=MESH)
    for step in range(1, NZ):
        for core in range(2):
            pl.semaphore_signal(barrier, inc=1, device_id=dest(s, step, core), device_id_type=MESH)
            peers += 1
    for axis in ("x", "y"):
        for by in (1, -1):
            pl.semaphore_signal(barrier, inc=1, device_id=s.peer(axis, by), device_id_type=MESH)
            peers += 1

    loads = [
        pltpu.make_async_copy(wg_ref.at[0], wcat.at[:, pl.ds(0, LANES)], wsem.at[0]),
        pltpu.make_async_copy(wu_ref.at[0], wcat.at[:, pl.ds(LANES, LANES)], wsem.at[1]),
        pltpu.make_async_copy(wd_ref.at[0], wdv, wsem.at[2]),
    ]
    for cp in loads:
        cp.start()

    def to_all(src_of, dst, ssem, rsem, chunks):
        for chunk in range(2):
            for pos in range(chunk * 8, chunk * 8 + 8):
                step = STEP_AT[pos]
                for core in range(2):
                    if step == 0 and core == 0:
                        src, dev = src_of(1 - s.c), sibling
                    elif step == 0:
                        continue
                    else:
                        src, dev = src_of(2 * pos + core), chunks(s, step, core)
                    send(src, dst(pos), ssem, rsem(chunk), dev, [])

    by_lane = slots_by_lane(routes_t_ref[...], s.z)
    rows = [g * MSG + t for g, t in by_lane]
    across = jnp.concatenate(
        [(g * RET + t).astype(F32) for g, t in by_lane] + [rw_t_ref[...], jnp.zeros((4, LANES), F32)], axis=0
    )
    down = across.T
    at = iota((32 * MSG, LANES), 0)
    cot32 = cot_ref[...].astype(F32)
    picks = jnp.concatenate(
        [
            ((at == rows[0]) | (at == rows[1])).astype(F32).astype(BF),
            (at == rows[0] + CAP).astype(F32).astype(BF),
            (at == rows[1] + CAP).astype(F32).astype(BF),
        ],
        axis=1,
    )
    stuff = jnp.concatenate(
        [x_ref[...]] + [(down[:, 2 + k : 3 + k] * cot32).astype(BF) for k in range(2)], axis=0
    )
    packed = dot(picks, stuff)
    for g in range(32):
        msg[g] = packed[g * MSG : (g + 1) * MSG, :].astype(BF)

    pl.semaphore_wait(barrier, peers)

    to_all(lambda k: msg.at[k], lambda pos: arrived.at[2 * pos + s.c], d_s, lambda c: d_r.at[c], dest)
    send(op_ref, opsib, o_s, o_r, sibling, log)
    arrived[pl.ds(s.c, 1)] = msg[pl.ds(s.c, 1)]

    gate = gate_ref[...].astype(F32)
    states = st_ref[...]
    root = 0.7978845608028654
    th = jnp.tanh(root * (gate + 0.044715 * (gate * gate * gate)))
    act_g = 0.5 * gate * (1.0 + th)
    act_v[...] = act_g
    dact_v[...] = 0.5 * (1.0 + th) + 0.5 * gate * (1.0 - th * th) * (root * (1.0 + 3 * 0.044715 * (gate * gate)))
    lanes_z = pl.ds(pl.multiple_of(s.z * LANES, LANES), LANES)
    mx[:, lanes_z] = turned((act_g * states).astype(BF).astype(F32)).astype(BF)
    landed(opsib, o_r)
    mine, other = op_ref[...].astype(F32), opsib[...].astype(F32)
    first = s.c == 0
    both = jnp.concatenate([jnp.where(first, mine, other), jnp.where(first, other, mine)], axis=0)
    both = turned(both)
    halfw = both.shape[0] // 2
    oprows = pl.ds(pl.multiple_of(s.c * halfw, 16), halfw)
    opt[oprows, lanes_z] = jnp.where(first, both[:halfw], both[halfw:]).astype(BF)

    def ring_part(z):
        lane = pl.ds(pl.multiple_of(z * LANES, LANES), LANES)
        return (opt.at[oprows, lane], mx.at[:, lane])

    ring = Ring(s, ring_part, ring_s, ring_r, log)
    ring.start()

    decays = jnp.exp(ld_ref[...])
    dec_v[...] = decays
    span = shifted_up(decays, 1, 1.0)
    for k in range(7):
        spans[k] = span
        span = span * shifted_up(span, 2**k, 1.0)
    spans[7] = span
    whole[s.sp] = span[0:1] * decays[0:1]
    lastrow[0] = states[127:128]
    to_all(lambda k: whole.at[s.sp], lambda pos: whole.at[s.sp], w_s, lambda c: w_r, dest)
    send(lastrow, prevrow, l_s, l_r, (lax.rem(s.sp + 1, 32), s.tp), log)

    ri = iota((2 * CHUNK, 16 * MSG), 0)
    ci = iota((2 * CHUNK, 16 * MSG), 1)
    second = ri >= CHUNK
    rr = jnp.where(second, ri - CHUNK, ri)
    squeeze = (ci == (rr // CAP) * MSG + rr % CAP + jnp.where(second, CAP, 0)).astype(F32).astype(BF)

    own = pl.ds(pl.multiple_of(s.tp * LANES, LANES), LANES)
    gathers = []
    for chunk in range(2):
        waited = arrived.at[pl.ds(0, 15)] if chunk == 0 else arrived.at[pl.ds(16, 16)]
        landed(waited, d_r.at[chunk])
        block = jnp.concatenate(
            [arrived[16 * chunk + i].astype(F32) for i in range(16)], axis=0
        ).astype(BF)
        tight = dot(squeeze, block).astype(BF)
        part = pl.ds(chunk * CHUNK, CHUNK)
        xr[part, own] = tight[:CHUNK]
        cr[part, own] = tight[CHUNK:]
        pair = []
        for n, (buf, u) in enumerate(((xr, "x"), (cr, "y"))):
            total = buf.at[part, pl.ds(0, 15 * LANES)]
            view = lane_blocks(buf, chunk * CHUNK, CHUNK)
            pair.append(PlaneGather(s, view, u, g_s.at[2 * chunk + n], g_r.at[2 * chunk + n], log, total))
        for g in pair:
            g.stage0()
        gathers.append(pair)
    for n, pair in enumerate(gathers):
        for k in range(1, 7):
            for g in pair:
                getattr(g, f"stage{k}")()
            if k % 2 == 0:
                ring.step(3 * n + k // 2 - 1)
    for cp in loads:
        cp.wait()

    saves = [
        pltpu.make_async_copy(xr, rows_out, osem.at[0]),
        pltpu.make_async_copy(cr, scaled_out, osem.at[1]),
    ]
    for cp in saves:
        cp.start()

    sums = [
        PlaneSum(s, terms, 0, "x", a1l, a1r, a2l, a2r, apart, aal, aar, abl, abr, None, q_s.at[0], q_r.at[0], log),
        PlaneSum(s, terms, CHUNK, "y", b1l, b1r, b2l, b2r, bpart, bal, bar, bbl, bbr, None, q_s.at[1], q_r.at[1], log),
    ]
    for chunk in range(2):
        part = pl.ds(chunk * CHUNK, CHUNK)
        pre = dot(xr[part, :], wcat[...])
        pgate, up = pre[:, :LANES], pre[:, LANES:]
        sig = jax.nn.sigmoid(pgate)
        act = pgate * sig
        slope = sig * (1.0 + pgate * (1.0 - sig))
        hid[part, :] = (act * up).astype(BF)
        gh = dot_t(cr[part, :], wdv[...])
        grads = jnp.concatenate([(gh * up * slope).astype(BF), (gh * act).astype(BF)], axis=1)
        gp[part, :] = grads
        for far in (2, 1, 3, 0):
            for i in range(2):
                places = []
                for k in (2 * i, 2 * i + 1):
                    if chunk == 0:
                        places.append((k, s.col("x", far)))
                    else:
                        places.append((s.col("y", far), k))
                w2 = jnp.concatenate(
                    [wcat[pl.ds(pl.multiple_of((a * 4 + b) * LANES, LANES), LANES), :] for a, b in places],
                    axis=0,
                )
                t2 = dot_t(grads, w2).astype(BF)
                for n, (a, b) in enumerate(places):
                    terms[a, b, part, :] = t2[:, n * LANES : (n + 1) * LANES]
            if far == 2:
                sums[chunk].stage0()
    saves += [
        pltpu.make_async_copy(gp, gp_out, osem.at[2]),
        pltpu.make_async_copy(hid, hidden_out, osem.at[3]),
    ]
    for cp in saves[2:]:
        cp.start()
    for k in range(1, 4):
        for q in sums:
            getattr(q, f"stage{k}")()
        if k < 3:
            ring.step(5 + k)
    send(opt.at[oprows, :], opt.at[oprows, :], h_s, h_r, sibling, log)

    ri = iota((16 * RET, CHUNK), 0)
    ci = iota((16 * RET, CHUNK), 1)
    spread = ((ri % RET < CAP) & (ci == (ri // RET) * CAP + ri % RET)).astype(F32).astype(BF)
    for chunk in range(2):
        total = sums[chunk].stage4()
        ret[pl.ds(16 * chunk, 16)] = dot(spread, total).astype(BF).reshape(16, RET, LANES)
    to_all(lambda k: ret.at[k], lambda pos: back.at[2 * pos + s.c], r_s, lambda c: r_r.at[c], origin)
    back[pl.ds(s.c, 1)] = ret[pl.ds(s.c, 1)]
    lane = iota((LANES, 32 * RET), 1)
    spots = down[:, 0:2].astype(I32)
    want = ((lane == spots[:, 0:1]) | (lane == spots[:, 1:2])).astype(F32).astype(BF)
    landed(back.at[pl.ds(0, 15)], r_r.at[0])
    landed(back.at[pl.ds(16, 16)], r_r.at[1])
    grown = dot(want, back[...].reshape(32 * RET, LANES))
    tok = (cot32 + grown).astype(BF)
    toks[:, own] = tok

    rows_of = toks.shape[0]
    fans = []
    for n, u in enumerate(("x", "y")):
        r0, cnt = n * (rows_of // 2), rows_of // 2
        total = toks.at[pl.ds(r0, cnt), pl.ds(0, 15 * LANES)]
        fans.append(PlaneGather(s, lane_blocks(toks, r0, cnt), u, t_s.at[n], t_r.at[n], log, total))
    for f in fans:
        f.stage0()
    inplace = s.z == s.tp
    odd = s.z % 2
    for q in range(8):
        col = 2 * q + odd
        src = toks.at[pl.ds(16 * q, 16), own]
        keep = jnp.logical_and(inplace, col == s.tp)

        @pl.when(jnp.logical_not(keep))
        def _():
            send(src, gt.at[s.z // 2, odd, q], x_s.at[q], x_r.at[s.z // 2], (2 * s.tp + s.c, col), [])

        @pl.when(keep)
        def _():
            gt[s.z // 2, odd, q] = src[...]

    turns = [
        PlaneGather(s, row_blocks(gt, 4 * n, 4), u, u_s.at[n], u_r.at[n], log)
        for n, u in enumerate(("x", "y"))
    ]
    for k in range(1, 4):
        for f in fans:
            getattr(f, f"stage{k}")()
    for i in range(8):
        keep = jnp.logical_and(inplace, s.z // 2 == i)

        @pl.when(jnp.logical_not(keep))
        def _():
            landed(gt.at[i, s.tp % 2, s.tp // 2], x_r.at[i])

    for f in turns:
        f.stage0()
    for k in range(4, 7):
        for f in fans:
            getattr(f, f"stage{k}")()
    landed(opt.at[pl.ds(pl.multiple_of((1 - s.c) * halfw, 16), halfw), :], h_r)
    gm = dot_t(toks[...], opt[...])
    act_g, decays, states = act_v[...], dec_v[...], st_ref[...]
    local = gm * act_g
    for k in range(7):
        local = local + spans[k] * shifted_up(local, 2**k, 0.0)
    ent[s.sp] = decays[0:1] * local[0:1]
    to_all(lambda k: ent.at[s.sp], lambda pos: ent.at[s.sp], e_s, lambda c: e_r, dest)
    ggb_out[...] = (gm * states * dact_v[...]).astype(BF)
    for k in range(1, 7):
        for f in turns:
            getattr(f, f"stage{k}")()
    gops[...] = dot(mx[...], gt[...].reshape(16 * LANES, LANES))
    send(gops, gopr, z_s, z_r, sibling, log)

    landed(whole.at[pl.ds(0, 31)], w_r)
    landed(prevrow, l_r)
    prev = jnp.where(s.sp == 0, 0.0, prevrow[0])
    prev = jnp.where(iota(states.shape, 0) == 0, prev, pltpu.roll(states, 1, 0)) * decays
    landed(ent.at[pl.ds(0, 31)], e_r)
    carry = jnp.zeros_like(decays[0:1])
    for k in range(31, 0, -1):
        carry = jnp.where(s.sp < k, ent[k] + whole[k] * carry, carry)
    full = local + spans[7] * carry
    git_out[...] = full
    gld_out[...] = (full * prev).astype(BF)
    landed(gopr, z_r)
    gop = turned(gops[...] + gopr[...])
    gop_out[...] = jnp.where(first, gop[:64], gop[64:])

    for cp in log:
        cp.wait_send()
    for q in range(8):
        keep = jnp.logical_and(inplace, 2 * q + odd == s.tp)

        @pl.when(jnp.logical_not(keep))
        def _():
            landed(toks.at[pl.ds(16 * q, 16), own], x_s.at[q])

    for g in gathers[0] + gathers[1] + fans + turns:
        g.drain()
    landed(msg.at[pl.ds(0, 31)], d_s)
    landed(ret.at[pl.ds(0, 31)], r_s)
    landed(ent.at[pl.ds(0, 31)], e_s)
    landed(whole.at[pl.ds(0, 31)], w_s)
    for cp in saves:
        cp.wait()


def step(x, cot, routes, rw, gate, ld, st, wg, wu, wd, op):
    vm = pl.BlockSpec(memory_space=pltpu.VMEM)
    hb = pl.BlockSpec(memory_space=pl.ANY)
    d = 16 * LANES
    w = gate.shape[1]
    V = pltpu.VMEM
    dma = pltpu.SemaphoreType.DMA
    S = jax.ShapeDtypeStruct
    sums = lambda: [
        V((4, HALF, LANES), BF), V((4, HALF, LANES), BF), V((4, CHUNK, LANES), BF), V((4, CHUNK, LANES), BF),
        V((4, CHUNK, LANES), BF),
        V((HALF, LANES), BF), V((HALF, LANES), BF), V((CHUNK, LANES), BF), V((CHUNK, LANES), BF),
    ]
    rows, scaled, gp, hidden, gop, ggb, gld, git = pl.pallas_call(
        body,
        out_shape=[
            S((ROWS, d), BF), S((ROWS, d), BF), S((ROWS, 2 * LANES), BF), S((ROWS, LANES), BF),
            S(op.shape, F32), S(gate.shape, BF), S(gate.shape, BF), S(gate.shape, F32),
        ],
        in_specs=[vm] * 8 + [hb] * 3,
        out_specs=[hb] * 4 + [vm] * 4,
        scratch_shapes=[
            V((32, MSG, LANES), BF), V((32, MSG, LANES), BF), V((ROWS, d), BF), V((ROWS, d), BF),
            V((d, 2 * LANES), BF), V((LANES, d), BF), V((ROWS, 2 * LANES), BF), V((ROWS, LANES), BF),
            V((4, 4, ROWS, LANES), BF), V((32, RET, LANES), BF), V((32, RET, LANES), BF),
            *sums(), *sums(),
            V(op.shape, BF), V((w, d), BF), V((w, d), BF), V((8, LANES, w), F32),
            V((LANES, w), F32), V((LANES, w), F32), V((LANES, w), F32), V((LANES, w), F32),
            V((LANES, d), BF), V((8, 2, 8, 16, LANES), BF), V((32, 1, w), F32), V((32, 1, w), F32),
            V((1, 1, w), F32), V((1, 1, w), F32), V((w, LANES), F32), V((w, LANES), F32),
            dma((3,)), dma((4,)), dma, dma((2,)), dma((4,)), dma((4, 20)),
            dma((2, 8)), dma((2, 8)), dma, dma((2,)),
            dma, dma, dma((2, 2, 8)), dma((2, 2, 8)), dma((2,)), dma((2, 20)), dma((2, 20)), dma((2, 20)),
            dma((8,)), dma((8,)), dma, dma, dma, dma, dma, dma, dma, dma, dma, dma,
        ],
        compiler_params=pltpu.CompilerParams(
            collective_id=0, has_side_effects=True, vmem_limit_bytes=56 * 1024 * 1024
        ),
        name="whole_step",
    )(x, cot, routes.T, rw.T, gate, ld, st, op, wg, wu, wd)

    def rows_by(a, b):
        return lax.dot_general(a, b, (((0,), (0,)), ((), ())), preferred_element_type=F32)

    return (
        rows_by(rows, gp[:, :LANES])[None], rows_by(rows, gp[:, LANES:])[None], rows_by(hidden, scaled)[None],
        gop, ggb, gld, git,
    )


def solution(mesh):
    both, rows = P("sp", "tp"), P("sp", None)
    last, middle = P("sp", None, "tp"), P("sp", "tp", None)
    return jax.shard_map(
        step,
        mesh=mesh,
        in_specs=(both, both, rows, rows, both, both, both, last, last, middle, both),
        out_specs=(last, last, middle, both, both, both, both),
        check_vma=False,
    )
```

time: 298 us -> 132 us (0.44)
  the two profiles are of different devices: /device:TPU:2 before, /device:TPU:1 now
where the time goes in v1:
time: 132 us; the launch traced here: 130 us
  Pallas kernels  116 us (88%)
  local copies, waits for them, and re-layouts  7.62 us (6%)
  matrix products  6.14 us (5%)
    pallas_call x1, Pallas kernels, step(): pl.pallas_call(body, out_shape=[S((ROWS, d), BF), S((ROWS, d), BF), S((RO...  116 us
    unnamed x19, local copies, waits for them, and re-layouts  7.62 us
    dot_general x3, matrix products, rows_by(): lax.dot_general(a, b, (((0,), (0,)), ((), ())), preferred_element_type=F32)  6.14 us

profile of v1, /device:TPU:1, one launch (start us, length us, event | category | flops | bytes accessed | tf_op | source)
XLA Modules:
  0.0 130.4 jit_solution(6830583513485284764)
XLA Ops:
  0.6 1.5 %copy.18.gate_ref = bf16[128,160]{1,0:T(8,128)(2,1)} copy(bf16[128,160]{0,1:T(8,128)(2,1)} %param.15) | data formatting | bytes 81920 | tf_op args[4]
  2.1 1.6 %copy.19.ld_ref = f32[128,160]{1,0:T(8,128)} copy(f32[128,160]{0,1:T(8,128)} %param.16) | data formatting | bytes 163840 | tf_op args[5]
  3.8 1.6 %copy.20.st_ref = f32[128,160]{1,0:T(8,128)} copy(f32[128,160]{0,1:T(8,128)} %param.17) | data formatting | bytes 163840 | tf_op args[6]
  5.4 116.0 %whole_step.1 = (bf16[320,2048]{1,0:T(8,128)(2,1)}, bf16[320,2048]{1,0:T(8,128)(2,1)}, bf16[320,256]{1,0:T(8,128)(2,1)}, bf16[320,128]{1,0:T(8,128)(2,1)}, f32[6...) custom-call(bf16[128,128]{1,0:T(8,128)(2,1)} %x_ref.1, ...), custom_call_target="tpu_custom_call" | custom-call | tf_op jit(solution)/shard_map/whole_step/pallas_call | solution.py:606
  121.4 0.0 copy-start.5
  121.4 0.0 copy-start.4
  121.4 0.0 copy-start.2
  121.4 0.0 copy-start
  121.4 0.0 copy-start.1
  121.5 2.9 %convolution_bitcast_fusion = f32[1,128,2048]{2,1,0:T(8,128)} fusion(bf16[320,128]{1,0:T(8,128)(2,1)} %get-tuple-element.17, bf16[320,2048]{1,0:T(8,128)(2,1)} %get-tuple-element.18), kind=kOutput, calls=%fused_computation | convolution fusion | flops 167772160 | bytes 2441216 | tf_op jit(solution)/shard_map/dot_general | solution.py:635
  124.4 0.0 copy-done.5
  124.4 0.7 copy.21
  125.1 0.0 copy-done.4
  125.1 0.7 copy.22
  125.8 0.0 copy-done.2
  125.8 0.7 copy.23
  126.6 0.0 copy-done
  126.6 0.0 copy-done.1
  126.6 1.6 %convolution_bitcast_fusion.1 = f32[1,2048,128]{2,1,0:T(8,128)} fusion(bf16[320,2048]{1,0:T(8,128)(2,1)S(1)} %copy-done, bf16[320,256]{1,0:T(8,128)(2,1)S(1)} %copy-done.1), kind=kOutput, calls=%fused_computation.1 | convolution fusion | flops 167772160 | bytes 2441216 | tf_op jit(solution)/shard_map/dot_general | solution.py:635
  128.2 0.0 copy-start.3
  128.2 1.6 %convolution_bitcast_fusion.2 = f32[1,2048,128]{2,1,0:T(8,128)} fusion(bf16[320,2048]{1,0:T(8,128)(2,1)S(1)} %copy-done, bf16[320,256]{1,0:T(8,128)(2,1)S(1)} %copy-done.1), kind=kOutput, calls=%fused_computation.2 | convolution fusion | flops 167772160 | bytes 2441216 | tf_op jit(solution)/shard_map/dot_general | solution.py:635
  129.8 0.0 copy-done.3
  129.8 0.6 copy.25
Async XLA Ops:
  121.4 3.0 %copy-start.5 = (bf16[128,160]{1,0:T(8,128)(2,1)S(1)}, bf16[128,160]{1,0:T(8,128)(2,1)}, u32[]{:S(2)}) copy-start(bf16[128,160]{1,0:T(8,128)(2,1)} %get-tuple-element.27) | copy-start | bytes 122884
  121.4 3.7 %copy-start.4 = (bf16[128,160]{1,0:T(8,128)(2,1)S(1)}, bf16[128,160]{1,0:T(8,128)(2,1)}, u32[]{:S(2)}) copy-start(bf16[128,160]{1,0:T(8,128)(2,1)} %get-tuple-element.28) | copy-start | bytes 122884
  121.4 4.4 %copy-start.2 = (f32[128,160]{1,0:T(8,128)S(1)}, f32[128,160]{1,0:T(8,128)}, u32[]{:S(2)}) copy-start(f32[128,160]{1,0:T(8,128)} %get-tuple-element.29) | copy-start | bytes 245764
  121.4 5.1 %copy-start = (bf16[320,2048]{1,0:T(8,128)(2,1)S(1)}, bf16[320,2048]{1,0:T(8,128)(2,1)}, u32[]{:S(2)}) copy-start(bf16[320,2048]{1,0:T(8,128)(2,1)} %get-tuple-element.15) | copy-start | bytes 3932164
  121.4 5.1 %copy-start.1 = (bf16[320,256]{1,0:T(8,128)(2,1)S(1)}, bf16[320,256]{1,0:T(8,128)(2,1)}, u32[]{:S(2)}) copy-start(bf16[320,256]{1,0:T(8,128)(2,1)} %get-tuple-element.16) | copy-start | bytes 491524
  128.2 1.6 %copy-start.3 = (f32[64,160]{1,0:T(8,128)S(1)}, f32[64,160]{1,0:T(8,128)}, u32[]{:S(2)}) copy-start(f32[64,160]{1,0:T(8,128)} %get-tuple-element.40) | copy-start | bytes 122884

commit v2 on v1

--- a/solution.py
+++ b/solution.py
@@ -19,6 +19,7 @@
 ROWS = 2 * NZ * CAP
 CHUNK = ROWS // 2
 HALF = CHUNK // 2
+VMEM_MIB = 30
 
 
 def place(step):
@@ -100,7 +101,6 @@
         view = self.view(0, 0)
         self.go(view, self.u, 1, 0)
         self.go(view, self.u, -1, 1)
-        self.fan(0)
 
     def stage1(self):
         landed(self.view(-1, 0), self.rsem.at[0])
@@ -140,6 +140,27 @@
     def drain(self):
         if self.total is not None:
             landed(self.total, self.ssem)
+
+
+class PlaneCast:
+    def __init__(self, spot, view, ssem, rsem):
+        self.s, self.view, self.ssem, self.rsem = spot, view, ssem, rsem
+        self.log = []
+        self.moves = [(dy, dx) for dy in (2, 1, 3, 0) for dx in (2, 1, 3, 0) if dy or dx]
+
+    def start(self):
+        block = self.view(self.s.tp, None)
+        for k, (dy, dx) in enumerate(self.moves):
+            dev = (self.s.sp, self.s.tpi("y", dy, dx))
+            send(block, block, self.ssem.at[k], self.rsem.at[k], dev, self.log)
+
+    def finish(self):
+        for k, (dy, dx) in enumerate(self.moves):
+            landed(self.view(self.s.tpi("y", -dy, -dx), None), self.rsem.at[k])
+
+    def drain(self):
+        for cp in self.log:
+            cp.wait_send()
 
 
 def lane_blocks(buf, r0, n):
@@ -267,11 +288,13 @@
     return [(group_of(routes_t[k : k + 1, :], z), slot[k]) for k in range(2)]
 
 
+def dot_0(a, b):
+    return lax.dot_general(a, b, (((0,), (0,)), ((), ())), preferred_element_type=F32)
+
+
 def shifted_up(v, by, fill):
-    n = v.shape[0]
-    if by % 8 == 0:
-        return jnp.concatenate([v[by:], jnp.full((by, v.shape[1]), fill, v.dtype)], axis=0)
-    return jnp.where(iota(v.shape, 0) < n - by, pltpu.roll(v, n - by, 0), fill)
+    n = v.shape[1]
+    return jnp.where(iota(v.shape, 1) < n - by, pltpu.roll(v, n - by, 1), fill)
 
 
 def turned(v):
@@ -283,16 +306,28 @@
 
 
 def body(
-    x_ref, cot_ref, routes_t_ref, rw_t_ref, gate_ref, ld_ref, st_ref, op_ref, wg_ref, wu_ref, wd_ref,
-    rows_out, scaled_out, gp_out, hidden_out, gop_out, ggb_out, gld_out, git_out,
+    x_in, cot_in, routes_in, rw_in, gate_in, ld_in, st_in, op_in, wg_ref, wu_ref, wd_ref,
+    gg_out, gu_out, gd_out, gop_out, ggb_out, gld_out, git_out,
+    x_ref, cot_ref, routes_t_ref, rw_t_ref, gate_ref, ld_ref, st_ref, op_ref,
     msg, arrived, xr, cr, wcat, wdv, gp, hid, terms, ret, back,
     a1l, a1r, a2l, a2r, apart, aal, aar, abl, abr,
     b1l, b1r, b2l, b2r, bpart, bal, bar, bbl, bbr,
-    opsib, mx, opt, spans, act_v, dact_v, dec_v, prev_v,
+    opsib, mx, opt, spans, act_v, dact_v, dec_v,
     toks, gt, ent, whole, lastrow, prevrow, gops, gopr,
-    wsem, osem, d_s, d_r, g_s, g_r, q_s, q_r, r_s, r_r,
+    isem, wsem, d_s, d_r, g_s, g_r, q_s, q_r, r_s, r_r,
     o_s, o_r, ring_s, ring_r, t_s, t_r, u_s, u_r, x_s, x_r, e_s, e_r, w_s, w_r, l_s, l_r, h_s, h_r, z_s, z_r,
 ):
+    inputs = [
+        pltpu.make_async_copy(src, dst, isem.at[k])
+        for k, (src, dst) in enumerate(
+            (
+                (routes_in, routes_t_ref), (rw_in, rw_t_ref), (x_in, x_ref), (cot_in, cot_ref),
+                (op_in, op_ref), (gate_in, gate_ref), (st_in, st_ref), (ld_in, ld_ref),
+            )
+        )
+    ]
+    for cp in inputs:
+        cp.start()
     s = Spot()
     log = []
     sibling = (2 * s.z + (1 - s.c), s.tp)
@@ -316,19 +351,21 @@
     for cp in loads:
         cp.start()
 
-    def to_all(src_of, dst, ssem, rsem, chunks):
-        for chunk in range(2):
-            for pos in range(chunk * 8, chunk * 8 + 8):
-                step = STEP_AT[pos]
-                for core in range(2):
-                    if step == 0 and core == 0:
-                        src, dev = src_of(1 - s.c), sibling
-                    elif step == 0:
+    def to_all(src_of, dst, ssem, rsem, target, chunk):
+        for pos in range(chunk * 8, chunk * 8 + 8):
+            step = STEP_AT[pos]
+            for turn in range(2):
+                core = (s.c, 1 - s.c)[turn]
+                if step == 0:
+                    if turn == 0:
                         continue
-                    else:
-                        src, dev = src_of(2 * pos + core), chunks(s, step, core)
-                    send(src, dst(pos), ssem, rsem(chunk), dev, [])
-
+                    dev = sibling
+                else:
+                    dev = target(s, step, core)
+                send(src_of(2 * pos + core), dst(pos), ssem, rsem, dev, [])
+
+    for cp in inputs[:2]:
+        cp.wait()
     by_lane = slots_by_lane(routes_t_ref[...], s.z)
     rows = [g * MSG + t for g, t in by_lane]
     across = jnp.concatenate(
@@ -336,6 +373,8 @@
     )
     down = across.T
     at = iota((32 * MSG, LANES), 0)
+    for cp in inputs[2:4]:
+        cp.wait()
     cot32 = cot_ref[...].astype(F32)
     picks = jnp.concatenate(
         [
@@ -354,7 +393,10 @@
 
     pl.semaphore_wait(barrier, peers)
 
-    to_all(lambda k: msg.at[k], lambda pos: arrived.at[2 * pos + s.c], d_s, lambda c: d_r.at[c], dest)
+    for chunk in range(2):
+        to_all(lambda k: msg.at[k], lambda pos: arrived.at[2 * pos + s.c], d_s, d_r.at[chunk], dest, chunk)
+    for cp in inputs[4:]:
+        cp.wait()
     send(op_ref, opsib, o_s, o_r, sibling, log)
     arrived[pl.ds(s.c, 1)] = msg[pl.ds(s.c, 1)]
 
@@ -366,7 +408,7 @@
     act_v[...] = act_g
     dact_v[...] = 0.5 * (1.0 + th) + 0.5 * gate * (1.0 - th * th) * (root * (1.0 + 3 * 0.044715 * (gate * gate)))
     lanes_z = pl.ds(pl.multiple_of(s.z * LANES, LANES), LANES)
-    mx[:, lanes_z] = turned((act_g * states).astype(BF).astype(F32)).astype(BF)
+    mx[:, lanes_z] = (act_g * states).astype(BF)
     landed(opsib, o_r)
     mine, other = op_ref[...].astype(F32), opsib[...].astype(F32)
     first = s.c == 0
@@ -390,9 +432,10 @@
         spans[k] = span
         span = span * shifted_up(span, 2**k, 1.0)
     spans[7] = span
-    whole[s.sp] = span[0:1] * decays[0:1]
-    lastrow[0] = states[127:128]
-    to_all(lambda k: whole.at[s.sp], lambda pos: whole.at[s.sp], w_s, lambda c: w_r, dest)
+    whole[s.sp] = turned(span * decays)[0:1]
+    lastrow[0] = turned(states)[LANES - 1 :]
+    for chunk in range(2):
+        to_all(lambda k: whole.at[s.sp], lambda pos: whole.at[s.sp], w_s, w_r, dest, chunk)
     send(lastrow, prevrow, l_s, l_r, (lax.rem(s.sp + 1, 32), s.tp), log)
 
     ri = iota((2 * CHUNK, 16 * MSG), 0)
@@ -403,7 +446,15 @@
 
     own = pl.ds(pl.multiple_of(s.tp * LANES, LANES), LANES)
     gathers = []
-    for chunk in range(2):
+    sums = [
+        PlaneSum(s, terms, 0, "x", a1l, a1r, a2l, a2r, apart, aal, aar, abl, abr, None, q_s.at[0], q_r.at[0], log),
+        PlaneSum(s, terms, CHUNK, "y", b1l, b1r, b2l, b2r, bpart, bal, bar, bbl, bbr, None, q_s.at[1], q_r.at[1], log),
+    ]
+    ri = iota((16 * RET, CHUNK), 0)
+    ci = iota((16 * RET, CHUNK), 1)
+    spread = ((ri % RET < CAP) & (ci == (ri // RET) * CAP + ri % RET)).astype(F32).astype(BF)
+
+    def enter(chunk):
         waited = arrived.at[pl.ds(0, 15)] if chunk == 0 else arrived.at[pl.ds(16, 16)]
         landed(waited, d_r.at[chunk])
         block = jnp.concatenate(
@@ -420,28 +471,18 @@
             pair.append(PlaneGather(s, view, u, g_s.at[2 * chunk + n], g_r.at[2 * chunk + n], log, total))
         for g in pair:
             g.stage0()
+        for g in pair:
+            g.fan(0)
         gathers.append(pair)
-    for n, pair in enumerate(gathers):
-        for k in range(1, 7):
-            for g in pair:
-                getattr(g, f"stage{k}")()
-            if k % 2 == 0:
-                ring.step(3 * n + k // 2 - 1)
-    for cp in loads:
-        cp.wait()
-
-    saves = [
-        pltpu.make_async_copy(xr, rows_out, osem.at[0]),
-        pltpu.make_async_copy(cr, scaled_out, osem.at[1]),
-    ]
-    for cp in saves:
-        cp.start()
-
-    sums = [
-        PlaneSum(s, terms, 0, "x", a1l, a1r, a2l, a2r, apart, aal, aar, abl, abr, None, q_s.at[0], q_r.at[0], log),
-        PlaneSum(s, terms, CHUNK, "y", b1l, b1r, b2l, b2r, bpart, bal, bar, bbl, bbr, None, q_s.at[1], q_r.at[1], log),
-    ]
-    for chunk in range(2):
+
+    def gather(chunk, k):
+        for g in gathers[chunk]:
+            getattr(g, f"stage{k}")()
+
+    def expert(chunk):
+        if chunk == 0:
+            for cp in loads:
+                cp.wait()
         part = pl.ds(chunk * CHUNK, CHUNK)
         pre = dot(xr[part, :], wcat[...])
         pgate, up = pre[:, :LANES], pre[:, LANES:]
@@ -469,27 +510,61 @@
                     terms[a, b, part, :] = t2[:, n * LANES : (n + 1) * LANES]
             if far == 2:
                 sums[chunk].stage0()
-    saves += [
-        pltpu.make_async_copy(gp, gp_out, osem.at[2]),
-        pltpu.make_async_copy(hid, hidden_out, osem.at[3]),
-    ]
-    for cp in saves[2:]:
-        cp.start()
-    for k in range(1, 4):
-        for q in sums:
-            getattr(q, f"stage{k}")()
-        if k < 3:
-            ring.step(5 + k)
-    send(opt.at[oprows, :], opt.at[oprows, :], h_s, h_r, sibling, log)
-
-    ri = iota((16 * RET, CHUNK), 0)
-    ci = iota((16 * RET, CHUNK), 1)
-    spread = ((ri % RET < CAP) & (ci == (ri // RET) * CAP + ri % RET)).astype(F32).astype(BF)
-    for chunk in range(2):
+
+    def summed(chunk, k):
+        getattr(sums[chunk], f"stage{k}")()
+
+    def leave(chunk):
         total = sums[chunk].stage4()
         ret[pl.ds(16 * chunk, 16)] = dot(spread, total).astype(BF).reshape(16, RET, LANES)
-    to_all(lambda k: ret.at[k], lambda pos: back.at[2 * pos + s.c], r_s, lambda c: r_r.at[c], origin)
+        to_all(lambda k: ret.at[k], lambda pos: back.at[2 * pos + s.c], r_s, r_r.at[chunk], origin, chunk)
+
+    def rung(k):
+        ring.step(k)
+
+    enter(0)
+    gather(0, 1)
+    enter(1)
+    rung(0)
+    gather(0, 2)
+    gather(0, 3)
+    gather(1, 1)
+    rung(1)
+    gather(0, 4)
+    gather(1, 2)
+    gather(0, 5)
+    gather(1, 3)
+    rung(2)
+    gather(0, 6)
+    expert(0)
+    gather(1, 4)
+    rung(3)
+    summed(0, 1)
+    gather(1, 5)
+    gather(1, 6)
+    summed(0, 2)
+    expert(1)
+    rung(4)
+    summed(0, 3)
+    summed(1, 1)
+    leave(0)
+    rung(5)
+    summed(1, 2)
+    summed(1, 3)
+    leave(1)
     back[pl.ds(s.c, 1)] = ret[pl.ds(s.c, 1)]
+    rung(6)
+
+    @pl.loop(0, 8)
+    def _(i):
+        lanes = pl.ds(pl.multiple_of(i * 2 * LANES, 2 * LANES), 2 * LANES)
+        block = dot_0(xr[:, lanes], gp[...])
+        gg_out[0, lanes, :] = block[:, :LANES]
+        gu_out[0, lanes, :] = block[:, LANES:]
+        gd_out[0, :, lanes] = dot_0(hid[...], cr[:, lanes])
+
+    rung(7)
+    send(opt.at[oprows, :], opt.at[oprows, :], h_s, h_r, sibling, log)
     lane = iota((LANES, 32 * RET), 1)
     spots = down[:, 0:2].astype(I32)
     want = ((lane == spots[:, 0:1]) | (lane == spots[:, 1:2])).astype(F32).astype(BF)
@@ -499,14 +574,6 @@
     tok = (cot32 + grown).astype(BF)
     toks[:, own] = tok
 
-    rows_of = toks.shape[0]
-    fans = []
-    for n, u in enumerate(("x", "y")):
-        r0, cnt = n * (rows_of // 2), rows_of // 2
-        total = toks.at[pl.ds(r0, cnt), pl.ds(0, 15 * LANES)]
-        fans.append(PlaneGather(s, lane_blocks(toks, r0, cnt), u, t_s.at[n], t_r.at[n], log, total))
-    for f in fans:
-        f.stage0()
     inplace = s.z == s.tp
     odd = s.z % 2
     for q in range(8):
@@ -522,13 +589,8 @@
         def _():
             gt[s.z // 2, odd, q] = src[...]
 
-    turns = [
-        PlaneGather(s, row_blocks(gt, 4 * n, 4), u, u_s.at[n], u_r.at[n], log)
-        for n, u in enumerate(("x", "y"))
-    ]
-    for k in range(1, 4):
-        for f in fans:
-            getattr(f, f"stage{k}")()
+    fans = PlaneCast(s, lane_blocks(toks, 0, toks.shape[0]), t_s, t_r)
+    fans.start()
     for i in range(8):
         keep = jnp.logical_and(inplace, s.z // 2 == i)
 
@@ -536,35 +598,32 @@
         def _():
             landed(gt.at[i, s.tp % 2, s.tp // 2], x_r.at[i])
 
-    for f in turns:
-        f.stage0()
-    for k in range(4, 7):
-        for f in fans:
-            getattr(f, f"stage{k}")()
+    turns = PlaneCast(s, row_blocks(gt, 0, 8), u_s, u_r)
+    turns.start()
     landed(opt.at[pl.ds(pl.multiple_of((1 - s.c) * halfw, 16), halfw), :], h_r)
-    gm = dot_t(toks[...], opt[...])
+    fans.finish()
+    gm = dot_t(opt[...], toks[...])
     act_g, decays, states = act_v[...], dec_v[...], st_ref[...]
     local = gm * act_g
     for k in range(7):
         local = local + spans[k] * shifted_up(local, 2**k, 0.0)
-    ent[s.sp] = decays[0:1] * local[0:1]
-    to_all(lambda k: ent.at[s.sp], lambda pos: ent.at[s.sp], e_s, lambda c: e_r, dest)
+    ent[s.sp] = turned(decays * local)[0:1]
+    for chunk in (1, 0):
+        to_all(lambda k: ent.at[s.sp], lambda pos: ent.at[s.sp], e_s, e_r, dest, chunk)
     ggb_out[...] = (gm * states * dact_v[...]).astype(BF)
-    for k in range(1, 7):
-        for f in turns:
-            getattr(f, f"stage{k}")()
+    turns.finish()
     gops[...] = dot(mx[...], gt[...].reshape(16 * LANES, LANES))
     send(gops, gopr, z_s, z_r, sibling, log)
 
     landed(whole.at[pl.ds(0, 31)], w_r)
     landed(prevrow, l_r)
-    prev = jnp.where(s.sp == 0, 0.0, prevrow[0])
-    prev = jnp.where(iota(states.shape, 0) == 0, prev, pltpu.roll(states, 1, 0)) * decays
+    prev = turned(jnp.broadcast_to(jnp.where(s.sp == 0, 0.0, prevrow[0]), (LANES, states.shape[0])))
+    prev = jnp.where(iota(states.shape, 1) == 0, prev, pltpu.roll(states, 1, 1)) * decays
     landed(ent.at[pl.ds(0, 31)], e_r)
-    carry = jnp.zeros_like(decays[0:1])
+    carry = jnp.zeros((1, states.shape[0]), F32)
     for k in range(31, 0, -1):
         carry = jnp.where(s.sp < k, ent[k] + whole[k] * carry, carry)
-    full = local + spans[7] * carry
+    full = local + spans[7] * turned(jnp.broadcast_to(carry, (LANES, states.shape[0])))
     git_out[...] = full
     gld_out[...] = (full * prev).astype(BF)
     landed(gopr, z_r)
@@ -580,19 +639,27 @@
         def _():
             landed(toks.at[pl.ds(16 * q, 16), own], x_s.at[q])
 
-    for g in gathers[0] + gathers[1] + fans + turns:
+    fans.drain()
+    turns.drain()
+    for g in gathers[0] + gathers[1]:
         g.drain()
     landed(msg.at[pl.ds(0, 31)], d_s)
     landed(ret.at[pl.ds(0, 31)], r_s)
     landed(ent.at[pl.ds(0, 31)], e_s)
     landed(whole.at[pl.ds(0, 31)], w_s)
-    for cp in saves:
+
+
+def settle(*refs):
+    copies = [pltpu.make_async_copy(refs[k], refs[7 + k], refs[14].at[k]) for k in range(7)]
+    for cp in copies:
+        cp.start()
+    for cp in copies:
         cp.wait()
 
 
 def step(x, cot, routes, rw, gate, ld, st, wg, wu, wd, op):
     vm = pl.BlockSpec(memory_space=pltpu.VMEM)
-    hb = pl.BlockSpec(memory_space=pl.ANY)
+    hb = pl.BlockSpec(memory_space=pltpu.MemorySpace.HBM)
     d = 16 * LANES
     w = gate.shape[1]
     V = pltpu.VMEM
@@ -603,41 +670,48 @@
         V((4, CHUNK, LANES), BF),
         V((HALF, LANES), BF), V((HALF, LANES), BF), V((CHUNK, LANES), BF), V((CHUNK, LANES), BF),
     ]
-    rows, scaled, gp, hidden, gop, ggb, gld, git = pl.pallas_call(
+    operands = (x, cot, routes.T, rw.T, gate.T, ld.T, st.T, op, wg, wu, wd)
+    gg, gu, gd, gop, ggb, gld, git = pl.pallas_call(
         body,
         out_shape=[
-            S((ROWS, d), BF), S((ROWS, d), BF), S((ROWS, 2 * LANES), BF), S((ROWS, LANES), BF),
-            S(op.shape, F32), S(gate.shape, BF), S(gate.shape, BF), S(gate.shape, F32),
+            S(wg.shape, F32), S(wu.shape, F32), S(wd.shape, F32),
+            S(op.shape, F32), S((w, LANES), BF), S((w, LANES), BF), S((w, LANES), F32),
         ],
-        in_specs=[vm] * 8 + [hb] * 3,
-        out_specs=[hb] * 4 + [vm] * 4,
+        in_specs=[hb] * 11,
+        out_specs=[vm] * 7,
         scratch_shapes=[
+            V(x.shape, BF), V(cot.shape, BF), V((2, LANES), I32), V((2, LANES), F32),
+            V((w, LANES), BF), V((w, LANES), F32), V((w, LANES), F32), V(op.shape, BF),
             V((32, MSG, LANES), BF), V((32, MSG, LANES), BF), V((ROWS, d), BF), V((ROWS, d), BF),
             V((d, 2 * LANES), BF), V((LANES, d), BF), V((ROWS, 2 * LANES), BF), V((ROWS, LANES), BF),
             V((4, 4, ROWS, LANES), BF), V((32, RET, LANES), BF), V((32, RET, LANES), BF),
             *sums(), *sums(),
-            V(op.shape, BF), V((w, d), BF), V((w, d), BF), V((8, LANES, w), F32),
-            V((LANES, w), F32), V((LANES, w), F32), V((LANES, w), F32), V((LANES, w), F32),
+            V(op.shape, BF), V((w, d), BF), V((w, d), BF), V((8, w, LANES), F32),
+            V((w, LANES), F32), V((w, LANES), F32), V((w, LANES), F32),
             V((LANES, d), BF), V((8, 2, 8, 16, LANES), BF), V((32, 1, w), F32), V((32, 1, w), F32),
             V((1, 1, w), F32), V((1, 1, w), F32), V((w, LANES), F32), V((w, LANES), F32),
-            dma((3,)), dma((4,)), dma, dma((2,)), dma((4,)), dma((4, 20)),
+            dma((8,)), dma((3,)), dma, dma((2,)), dma((4,)), dma((4, 20)),
             dma((2, 8)), dma((2, 8)), dma, dma((2,)),
-            dma, dma, dma((2, 2, 8)), dma((2, 2, 8)), dma((2,)), dma((2, 20)), dma((2, 20)), dma((2, 20)),
+            dma, dma, dma((2, 2, 8)), dma((2, 2, 8)), dma((16,)), dma((16,)), dma((16,)), dma((16,)),
             dma((8,)), dma((8,)), dma, dma, dma, dma, dma, dma, dma, dma, dma, dma,
         ],
         compiler_params=pltpu.CompilerParams(
-            collective_id=0, has_side_effects=True, vmem_limit_bytes=56 * 1024 * 1024
+            collective_id=0, has_side_effects=True, vmem_limit_bytes=VMEM_MIB * 1024 * 1024
         ),
         name="whole_step",
-    )(x, cot, routes.T, rw.T, gate, ld, st, op, wg, wu, wd)
-
-    def rows_by(a, b):
-        return lax.dot_general(a, b, (((0,), (0,)), ((), ())), preferred_element_type=F32)
-
-    return (
-        rows_by(rows, gp[:, :LANES])[None], rows_by(rows, gp[:, LANES:])[None], rows_by(hidden, scaled)[None],
-        gop, ggb, gld, git,
-    )
+    )(*[pltpu.with_memory_space_constraint(a, pltpu.MemorySpace.HBM) for a in operands])
+
+    outs = (gg, gu, gd, gop, ggb, gld, git)
+    gg, gu, gd, gop, ggb, gld, git = pl.pallas_call(
+        settle,
+        out_shape=[S(o.shape, o.dtype) for o in outs],
+        in_specs=[vm] * 7,
+        out_specs=[hb] * 7,
+        scratch_shapes=[dma((7,))],
+        compiler_params=pltpu.CompilerParams(vmem_limit_bytes=4 * 1024 * 1024),
+        name="settle",
+    )(*outs)
+    return gg, gu, gd, gop, ggb.T, gld.T, git.T
 
 
 def solution(mesh):

time: 132 us -> 102 us (0.77); the launches traced: 130 us -> 102 us
  Pallas kernels: 116 us -> 101 us
  local copies, waits for them, and re-layouts: 7.62 us -> 0 us
  matrix products: 6.14 us -> 0 us
    pallas_call x1 -> x2, Pallas kernels: 116 us -> 101 us  [the longest x1 99.4 us: step(): pl.pallas_call(body, out_shape=[S(wg.shape, F32), S(wu.shape, F32), S(wd....]
    unnamed x19 -> x0, local copies, waits for them, and re-layouts: 7.62 us -> none
    dot_general x3 -> x0, matrix products: 6.14 us -> none  [rows_by(): lax.dot_general(a, b, (((0,), (0,)), ((), ())), preferred_element_type=F32)]
where the time goes in v2:
time: 102 us
  Pallas kernels  101 us (99%)
    pallas_call x1, Pallas kernels, step(): pl.pallas_call(body, out_shape=[S(wg.shape, F32), S(wu.shape, F32), S(wd....  99.4 us

profile of v2, /device:TPU:1, one launch (start us, length us, event | category | flops | bytes accessed | tf_op | source)
XLA Modules:
  0.0 101.8 jit_solution(6621219841559051761)
XLA Ops:
  0.6 99.4 %whole_step.1 = (f32[1,2048,128]{2,1,0:T(8,128)S(1)}, f32[1,2048,128]{2,1,0:T(8,128)S(1)}, f32[1,128,2048]{2,1,0:T(8,128)S(1)}, f32[64,160]{1,0:T(8,128)S(1)}, b...) custom-call(bf16[128,128]{1,0:T(8,128)(2,1)} %x_in.1, bf16[128,128]{1,0:T(8,128)(2,1)} %cot_in.1, ...), custom_call_target="tpu_custom_call" | custom-call | tf_op jit(solution)/shard_map/whole_step/pallas_call | solution.py:674
  100.1 1.8 %settle.1 = (f32[1,2048,128]{2,1,0:T(8,128)}, f32[1,2048,128]{2,1,0:T(8,128)}, f32[1,128,2048]{2,1,0:T(8,128)}, f32[64,160]{1,0:T(8,128)}, bf16[160,128]{1,0:T(8...) custom-call(f32[1,2048,128]{2,1,0:T(8,128)S(1)} %get-tuple-element.21.refs_0_, ...), custom_call_target="tpu_custom_call" | custom-call | tf_op jit(solution)/shard_map/settle/pallas_call | solution.py:705

commit v3 on v2

--- a/solution.py
+++ b/solution.py
@@ -76,91 +76,60 @@
 
 
 class PlaneGather:
-    def __init__(self, spot, view, u, ssem, rsem, log, total=None):
+    def __init__(self, spot, view, u, ssem, rsem, buf, rows):
         self.s, self.block, self.u = spot, view, u
         self.v = "y" if u == "x" else "x"
-        self.ssem, self.rsem, self.log, self.total = ssem, rsem, log, total
-        self.sent = 0
+        self.ssem, self.rsem, self.buf, self.rows = ssem, rsem, buf, rows
         self.fu = (0, -1, 1, 2)
 
     def view(self, du, dv, half=None):
         return self.block(self.s.tpi(self.u, du, dv), half)
 
     def go(self, view, axis, by, k):
-        ssem = self.ssem.at[self.sent] if self.total is None else self.ssem
-        log = self.log if self.total is None else []
-        send(view, view, ssem, self.rsem.at[k], self.s.peer(axis, by), log)
-        self.sent += 1
+        send(view, view, self.ssem, self.rsem.at[k], self.s.peer(axis, by), [])
 
     def fan(self, j):
         view = self.view(self.fu[j], 0)
-        self.go(view, self.v, 1, 4 + 4 * j)
-        self.go(view, self.v, -1, 5 + 4 * j)
+        for by in (1, -1, 2):
+            self.go(view, self.v, by, 3)
 
     def stage0(self):
         view = self.view(0, 0)
-        self.go(view, self.u, 1, 0)
-        self.go(view, self.u, -1, 1)
+        for k, by in enumerate((1, -1, 2)):
+            self.go(view, self.u, by, k)
 
     def stage1(self):
-        landed(self.view(-1, 0), self.rsem.at[0])
-        self.go(self.view(-1, 0, 0), self.u, 1, 2)
-        self.fan(1)
-        landed(self.view(1, 0), self.rsem.at[1])
-        self.go(self.view(1, 0, 1), self.u, -1, 3)
-        self.fan(2)
-
-    def relay(self, j):
-        du = self.fu[j]
-        landed(self.view(du, -1), self.rsem.at[4 + 4 * j])
-        self.go(self.view(du, -1, 0), self.v, 1, 6 + 4 * j)
-        landed(self.view(du, 1), self.rsem.at[5 + 4 * j])
-        self.go(self.view(du, 1, 1), self.v, -1, 7 + 4 * j)
+        for j in (1, 2):
+            landed(self.view(self.fu[j], 0), self.rsem.at[j - 1])
+            self.fan(j)
 
     def stage2(self):
-        self.relay(0)
+        landed(self.view(2, 0), self.rsem.at[2])
+        self.fan(3)
 
     def stage3(self):
-        landed(self.view(2, 0, 0), self.rsem.at[2])
-        landed(self.view(2, 0, 1), self.rsem.at[3])
-        self.fan(3)
-
-    def stage4(self):
-        self.relay(1)
-        self.relay(2)
-
-    def stage5(self):
-        self.relay(3)
-
-    def stage6(self):
-        for j in range(4):
-            landed(self.view(self.fu[j], 2, 0), self.rsem.at[6 + 4 * j])
-            landed(self.view(self.fu[j], 2, 1), self.rsem.at[7 + 4 * j])
+        landed(self.buf.at[self.rows, pl.ds(0, 12 * LANES)], self.rsem.at[3])
 
     def drain(self):
-        if self.total is not None:
-            landed(self.total, self.ssem)
+        landed(self.buf.at[self.rows, pl.ds(0, 15 * LANES)], self.ssem)
 
 
 class PlaneCast:
-    def __init__(self, spot, view, ssem, rsem):
-        self.s, self.view, self.ssem, self.rsem = spot, view, ssem, rsem
-        self.log = []
+    def __init__(self, spot, view, ssem, rsem, total):
+        self.s, self.view, self.ssem, self.rsem, self.total = spot, view, ssem, rsem, total
         self.moves = [(dy, dx) for dy in (2, 1, 3, 0) for dx in (2, 1, 3, 0) if dy or dx]
 
     def start(self):
         block = self.view(self.s.tp, None)
-        for k, (dy, dx) in enumerate(self.moves):
+        for dy, dx in self.moves:
             dev = (self.s.sp, self.s.tpi("y", dy, dx))
-            send(block, block, self.ssem.at[k], self.rsem.at[k], dev, self.log)
+            send(block, block, self.ssem, self.rsem, dev, [])
 
     def finish(self):
-        for k, (dy, dx) in enumerate(self.moves):
-            landed(self.view(self.s.tpi("y", -dy, -dx), None), self.rsem.at[k])
+        landed(self.total, self.rsem)
 
     def drain(self):
-        for cp in self.log:
-            cp.wait_send()
+        landed(self.total, self.ssem)
 
 
 def lane_blocks(buf, r0, n):
@@ -183,8 +152,8 @@
 
 
 class Ring:
-    def __init__(self, spot, part, ssem, rsem, log):
-        self.s, self.part, self.ssem, self.rsem, self.log = spot, part, ssem, rsem, log
+    def __init__(self, spot, part, ssem, rsem):
+        self.s, self.part, self.ssem, self.rsem = spot, part, ssem, rsem
 
     def at(self, by):
         return lax.rem(self.s.z + (by + NZ), NZ)
@@ -192,8 +161,8 @@
     def go(self, way, k):
         by = 1 if way == 0 else -1
         dev = (2 * self.at(by) + self.s.c, self.s.tp)
-        for n, view in enumerate(self.part(self.at(-by * k))):
-            send(view, view, self.ssem.at[way, n, k], self.rsem.at[way, n, k], dev, self.log)
+        view = self.part(self.at(-by * k))
+        send(view, view, self.ssem, self.rsem.at[way, k], dev, [])
 
     def start(self):
         self.go(0, 0)
@@ -202,65 +171,45 @@
     def step(self, k):
         for way, by, last in ((0, 1, 8), (1, -1, 7)):
             if k < last:
-                for n, view in enumerate(self.part(self.at(-by * (k + 1)))):
-                    landed(view, self.rsem.at[way, n, k])
+                landed(self.part(self.at(-by * (k + 1))), self.rsem.at[way, k])
                 if k + 1 < last:
                     self.go(way, k + 1)
 
 
 class PlaneSum:
-    def __init__(self, spot, buf, r0, u, one_l, one_r, two_l, two_r, part, a_l, a_r, b_l, b_r, tmp, ssem, rsem, log):
+    def __init__(self, spot, buf, r0, u, one, part, two, ssem, rsem):
         self.s, self.buf, self.r0, self.u = spot, buf, r0, u
         self.v = "y" if u == "x" else "x"
-        self.one = (one_l, one_r)
-        self.two = (two_l, two_r)
-        self.part, self.a, self.b, self.tmp = part, (a_l, a_r), (b_l, b_r), tmp
-        self.ssem, self.rsem, self.log = ssem, rsem, log
-
-    def block(self, du, r0, n):
+        self.one, self.part, self.two = one, part, two
+        self.ssem, self.rsem = ssem, rsem
+
+    def block(self, du):
         a = self.s.col(self.u, du)
         if self.u == "x":
-            return self.buf.at[:, a, pl.ds(r0, n), :]
-        return self.buf.at[a, :, pl.ds(r0, n), :]
+            return self.buf.at[:, a, pl.ds(self.r0, HALF), :]
+        return self.buf.at[a, :, pl.ds(self.r0, HALF), :]
 
     def go(self, src, dst, axis, by, k):
-        send(src, dst, self.ssem.at[k], self.rsem.at[k], self.s.peer(axis, by), self.log)
+        send(src, dst, self.ssem, self.rsem.at[k], self.s.peer(axis, by), [])
 
     def stage0(self):
-        self.go(self.block(2, self.r0, HALF), self.one[0], self.u, 1, 0)
-        self.go(self.block(2, self.r0 + HALF, HALF), self.one[1], self.u, -1, 1)
+        for k, by in enumerate((2, 1, -1)):
+            self.go(self.block(by), self.one.at[k], self.u, by, 0)
 
     def stage1(self):
-        for side, by in ((0, 1), (1, -1)):
-            landed(self.one[side], self.rsem.at[side])
-            mine = self.block(by, self.r0 + side * HALF, HALF)
-            mine[...] = (mine[...].astype(F32) + self.one[side][...].astype(F32)).astype(BF)
-            self.go(self.block(by, self.r0, CHUNK), self.two[side], self.u, by, 2 + side)
+        total = self.block(0)[...].astype(F32)
+        landed(self.one, self.rsem.at[0])
+        for k in range(3):
+            total = total + self.one[k].astype(F32)
+        self.part[...] = total.astype(BF)
+        for k, by in enumerate((2, 1, -1)):
+            self.go(self.part.at[self.s.col(self.v, by)], self.two.at[k], self.v, by, 1)
 
     def stage2(self):
-        landed(self.two[0], self.rsem.at[2])
-        landed(self.two[1], self.rsem.at[3])
-        own = self.block(0, self.r0, CHUNK)
-        self.part[...] = (
-            own[...].astype(F32) + self.two[0][...].astype(F32) + self.two[1][...].astype(F32)
-        ).astype(BF)
-        far = self.s.col(self.v, 2)
-        self.go(self.part.at[far, pl.ds(0, HALF), :], self.a[0], self.v, 1, 4)
-        self.go(self.part.at[far, pl.ds(HALF, HALF), :], self.a[1], self.v, -1, 5)
-
-    def stage3(self):
-        for side, by in ((0, 1), (1, -1)):
-            landed(self.a[side], self.rsem.at[4 + side])
-            near = self.s.col(self.v, by)
-            mine = self.part.at[near, pl.ds(side * HALF, HALF), :]
-            mine[...] = (mine[...].astype(F32) + self.a[side][...].astype(F32)).astype(BF)
-            self.go(self.part.at[near], self.b[side], self.v, by, 6 + side)
-
-    def stage4(self):
-        landed(self.b[0], self.rsem.at[6])
-        landed(self.b[1], self.rsem.at[7])
-        own = self.part[self.s.col(self.v, 0)]
-        total = own.astype(F32) + self.b[0][...].astype(F32) + self.b[1][...].astype(F32)
+        total = self.part[self.s.col(self.v, 0)].astype(F32)
+        landed(self.two, self.rsem.at[1])
+        for k in range(3):
+            total = total + self.two[k].astype(F32)
         return total.astype(BF)
 
 
@@ -310,9 +259,8 @@
     gg_out, gu_out, gd_out, gop_out, ggb_out, gld_out, git_out,
     x_ref, cot_ref, routes_t_ref, rw_t_ref, gate_ref, ld_ref, st_ref, op_ref,
     msg, arrived, xr, cr, wcat, wdv, gp, hid, terms, ret, back,
-    a1l, a1r, a2l, a2r, apart, aal, aar, abl, abr,
-    b1l, b1r, b2l, b2r, bpart, bal, bar, bbl, bbr,
-    opsib, mx, opt, spans, act_v, dact_v, dec_v,
+    one, part_v, two,
+    opsib, mo, osib, spans, act_v, dact_v, dec_v, lead_v,
     toks, gt, ent, whole, lastrow, prevrow, gops, gopr,
     isem, wsem, d_s, d_r, g_s, g_r, q_s, q_r, r_s, r_r,
     o_s, o_r, ring_s, ring_r, t_s, t_r, u_s, u_r, x_s, x_r, e_s, e_r, w_s, w_r, l_s, l_r, h_s, h_r, z_s, z_r,
@@ -339,7 +287,7 @@
             pl.semaphore_signal(barrier, inc=1, device_id=dest(s, step, core), device_id_type=MESH)
             peers += 1
     for axis in ("x", "y"):
-        for by in (1, -1):
+        for by in (1, -1, 2):
             pl.semaphore_signal(barrier, inc=1, device_id=s.peer(axis, by), device_id_type=MESH)
             peers += 1
 
@@ -352,7 +300,7 @@
         cp.start()
 
     def to_all(src_of, dst, ssem, rsem, target, chunk):
-        for pos in range(chunk * 8, chunk * 8 + 8):
+        for pos in range(8) if chunk == 0 else range(15, 7, -1):
             step = STEP_AT[pos]
             for turn in range(2):
                 core = (s.c, 1 - s.c)[turn]
@@ -400,6 +348,8 @@
     send(op_ref, opsib, o_s, o_r, sibling, log)
     arrived[pl.ds(s.c, 1)] = msg[pl.ds(s.c, 1)]
 
+    width = gate_ref.shape[0]
+    halfw = width // 2
     gate = gate_ref[...].astype(F32)
     states = st_ref[...]
     root = 0.7978845608028654
@@ -408,21 +358,19 @@
     act_v[...] = act_g
     dact_v[...] = 0.5 * (1.0 + th) + 0.5 * gate * (1.0 - th * th) * (root * (1.0 + 3 * 0.044715 * (gate * gate)))
     lanes_z = pl.ds(pl.multiple_of(s.z * LANES, LANES), LANES)
-    mx[:, lanes_z] = (act_g * states).astype(BF)
+    mo[pl.ds(0, width), lanes_z] = (act_g * states).astype(BF)
     landed(opsib, o_r)
     mine, other = op_ref[...].astype(F32), opsib[...].astype(F32)
     first = s.c == 0
     both = jnp.concatenate([jnp.where(first, mine, other), jnp.where(first, other, mine)], axis=0)
     both = turned(both)
-    halfw = both.shape[0] // 2
-    oprows = pl.ds(pl.multiple_of(s.c * halfw, 16), halfw)
-    opt[oprows, lanes_z] = jnp.where(first, both[:halfw], both[halfw:]).astype(BF)
+    oprows = pl.ds(width, halfw)
+    mo[oprows, lanes_z] = jnp.where(first, both[:halfw], both[halfw:]).astype(BF)
 
     def ring_part(z):
-        lane = pl.ds(pl.multiple_of(z * LANES, LANES), LANES)
-        return (opt.at[oprows, lane], mx.at[:, lane])
-
-    ring = Ring(s, ring_part, ring_s, ring_r, log)
+        return mo.at[:, pl.ds(pl.multiple_of(z * LANES, LANES), LANES)]
+
+    ring = Ring(s, ring_part, ring_s, ring_r)
     ring.start()
 
     decays = jnp.exp(ld_ref[...])
@@ -433,6 +381,10 @@
         span = span * shifted_up(span, 2**k, 1.0)
     spans[7] = span
     whole[s.sp] = turned(span * decays)[0:1]
+    lead = decays
+    for k in range(7):
+        lead = lead * jnp.where(iota(lead.shape, 1) >= 2**k, pltpu.roll(lead, 2**k, 1), 1.0)
+    lead_v[...] = lead
     lastrow[0] = turned(states)[LANES - 1 :]
     for chunk in range(2):
         to_all(lambda k: whole.at[s.sp], lambda pos: whole.at[s.sp], w_s, w_r, dest, chunk)
@@ -447,8 +399,14 @@
     own = pl.ds(pl.multiple_of(s.tp * LANES, LANES), LANES)
     gathers = []
     sums = [
-        PlaneSum(s, terms, 0, "x", a1l, a1r, a2l, a2r, apart, aal, aar, abl, abr, None, q_s.at[0], q_r.at[0], log),
-        PlaneSum(s, terms, CHUNK, "y", b1l, b1r, b2l, b2r, bpart, bal, bar, bbl, bbr, None, q_s.at[1], q_r.at[1], log),
+        [
+            PlaneSum(
+                s, terms, chunk * CHUNK + n * HALF, u, one.at[chunk, n], part_v.at[chunk, n], two.at[chunk, n],
+                q_s.at[chunk, n], q_r.at[chunk, n],
+            )
+            for n, u in enumerate(("x", "y"))
+        ]
+        for chunk in range(2)
     ]
     ri = iota((16 * RET, CHUNK), 0)
     ci = iota((16 * RET, CHUNK), 1)
@@ -466,9 +424,8 @@
         cr[part, own] = tight[CHUNK:]
         pair = []
         for n, (buf, u) in enumerate(((xr, "x"), (cr, "y"))):
-            total = buf.at[part, pl.ds(0, 15 * LANES)]
             view = lane_blocks(buf, chunk * CHUNK, CHUNK)
-            pair.append(PlaneGather(s, view, u, g_s.at[2 * chunk + n], g_r.at[2 * chunk + n], log, total))
+            pair.append(PlaneGather(s, view, u, g_s.at[2 * chunk + n], g_r.at[2 * chunk + n], buf, part))
         for g in pair:
             g.stage0()
         for g in pair:
@@ -493,29 +450,19 @@
         gh = dot_t(cr[part, :], wdv[...])
         grads = jnp.concatenate([(gh * up * slope).astype(BF), (gh * act).astype(BF)], axis=1)
         gp[part, :] = grads
-        for far in (2, 1, 3, 0):
-            for i in range(2):
-                places = []
-                for k in (2 * i, 2 * i + 1):
-                    if chunk == 0:
-                        places.append((k, s.col("x", far)))
-                    else:
-                        places.append((s.col("y", far), k))
-                w2 = jnp.concatenate(
-                    [wcat[pl.ds(pl.multiple_of((a * 4 + b) * LANES, LANES), LANES), :] for a, b in places],
-                    axis=0,
-                )
-                t2 = dot_t(grads, w2).astype(BF)
-                for n, (a, b) in enumerate(places):
-                    terms[a, b, part, :] = t2[:, n * LANES : (n + 1) * LANES]
-            if far == 2:
-                sums[chunk].stage0()
-
-    def summed(chunk, k):
-        getattr(sums[chunk], f"stage{k}")()
+        for i in range(8):
+            t2 = dot_t(grads, wcat[pl.ds(2 * i * LANES, 2 * LANES), :]).astype(BF)
+            terms[i // 2, 2 * (i % 2), part, :] = t2[:, :LANES]
+            terms[i // 2, 2 * (i % 2) + 1, part, :] = t2[:, LANES:]
+        for q in sums[chunk]:
+            q.stage0()
+
+    def summed(chunk):
+        for q in sums[chunk]:
+            q.stage1()
 
     def leave(chunk):
-        total = sums[chunk].stage4()
+        total = jnp.concatenate([q.stage2() for q in sums[chunk]], axis=0)
         ret[pl.ds(16 * chunk, 16)] = dot(spread, total).astype(BF).reshape(16, RET, LANES)
         to_all(lambda k: ret.at[k], lambda pos: back.at[2 * pos + s.c], r_s, r_r.at[chunk], origin, chunk)
 
@@ -524,36 +471,25 @@
 
     enter(0)
     gather(0, 1)
+    gather(0, 2)
     enter(1)
     rung(0)
-    gather(0, 2)
+    gather(1, 1)
     gather(0, 3)
-    gather(1, 1)
     rung(1)
-    gather(0, 4)
     gather(1, 2)
-    gather(0, 5)
+    expert(0)
     gather(1, 3)
     rung(2)
-    gather(0, 6)
-    expert(0)
-    gather(1, 4)
+    expert(1)
+    summed(0)
     rung(3)
-    summed(0, 1)
-    gather(1, 5)
-    gather(1, 6)
-    summed(0, 2)
-    expert(1)
+    summed(1)
+    leave(0)
     rung(4)
-    summed(0, 3)
-    summed(1, 1)
-    leave(0)
-    rung(5)
-    summed(1, 2)
-    summed(1, 3)
     leave(1)
     back[pl.ds(s.c, 1)] = ret[pl.ds(s.c, 1)]
-    rung(6)
+    rung(5)
 
     @pl.loop(0, 8)
     def _(i):
@@ -563,8 +499,7 @@
         gu_out[0, lanes, :] = block[:, LANES:]
         gd_out[0, :, lanes] = dot_0(hid[...], cr[:, lanes])
 
-    rung(7)
-    send(opt.at[oprows, :], opt.at[oprows, :], h_s, h_r, sibling, log)
+    rung(6)
     lane = iota((LANES, 32 * RET), 1)
     spots = down[:, 0:2].astype(I32)
     want = ((lane == spots[:, 0:1]) | (lane == spots[:, 1:2])).astype(F32).astype(BF)
@@ -574,6 +509,14 @@
     tok = (cot32 + grown).astype(BF)
     toks[:, own] = tok
 
+    fans = []
+    for n, u in enumerate(("x", "y")):
+        r0, cnt = n * (toks.shape[0] // 2), toks.shape[0] // 2
+        fans.append(PlaneGather(s, lane_blocks(toks, r0, cnt), u, t_s.at[n], t_r.at[n], toks, pl.ds(r0, cnt)))
+    for f in fans:
+        f.stage0()
+    for f in fans:
+        f.fan(0)
     inplace = s.z == s.tp
     odd = s.z % 2
     for q in range(8):
@@ -583,36 +526,42 @@
 
         @pl.when(jnp.logical_not(keep))
         def _():
-            send(src, gt.at[s.z // 2, odd, q], x_s.at[q], x_r.at[s.z // 2], (2 * s.tp + s.c, col), [])
+            send(src, gt.at[s.z // 2, odd, q], x_s, x_r, (2 * s.tp + s.c, col), [])
 
         @pl.when(keep)
         def _():
             gt[s.z // 2, odd, q] = src[...]
 
-    fans = PlaneCast(s, lane_blocks(toks, 0, toks.shape[0]), t_s, t_r)
-    fans.start()
-    for i in range(8):
-        keep = jnp.logical_and(inplace, s.z // 2 == i)
-
-        @pl.when(jnp.logical_not(keep))
+    def turned_in(sem):
+        @pl.when(inplace)
         def _():
-            landed(gt.at[i, s.tp % 2, s.tp // 2], x_r.at[i])
-
-    turns = PlaneCast(s, row_blocks(gt, 0, 8), u_s, u_r)
-    turns.start()
-    landed(opt.at[pl.ds(pl.multiple_of((1 - s.c) * halfw, 16), halfw), :], h_r)
-    fans.finish()
-    gm = dot_t(opt[...], toks[...])
+            landed(toks.at[pl.ds(0, 112), own], sem)
+
+        @pl.when(jnp.logical_not(inplace))
+        def _():
+            landed(toks.at[pl.ds(0, 128), own], sem)
+
+    rung(7)
+    send(mo.at[oprows, :], osib, h_s, h_r, sibling, log)
+    for k in (1, 2, 3):
+        for f in fans:
+            getattr(f, f"stage{k}")()
+    landed(osib, h_r)
+    halves = (dot_t(mo[oprows, :], toks[...]), dot_t(osib[...], toks[...]))
+    gm = jnp.concatenate([jnp.where(first, halves[0], halves[1]), jnp.where(first, halves[1], halves[0])], axis=0)
     act_g, decays, states = act_v[...], dec_v[...], st_ref[...]
     local = gm * act_g
+    ent[s.sp] = jnp.sum(turned(lead_v[...] * local), axis=0, keepdims=True)
+    for chunk in (1, 0):
+        to_all(lambda k: ent.at[s.sp], lambda pos: ent.at[s.sp], e_s, e_r, dest, chunk)
+    turned_in(x_r)
+    turns = PlaneCast(s, row_blocks(gt, 0, 8), u_s, u_r, toks.at[:, pl.ds(0, 15 * LANES)])
+    turns.start()
     for k in range(7):
         local = local + spans[k] * shifted_up(local, 2**k, 0.0)
-    ent[s.sp] = turned(decays * local)[0:1]
-    for chunk in (1, 0):
-        to_all(lambda k: ent.at[s.sp], lambda pos: ent.at[s.sp], e_s, e_r, dest, chunk)
     ggb_out[...] = (gm * states * dact_v[...]).astype(BF)
     turns.finish()
-    gops[...] = dot(mx[...], gt[...].reshape(16 * LANES, LANES))
+    gops[...] = dot(mo[pl.ds(0, width), :], gt[...].reshape(16 * LANES, LANES))
     send(gops, gopr, z_s, z_r, sibling, log)
 
     landed(whole.at[pl.ds(0, 31)], w_r)
@@ -632,17 +581,13 @@
 
     for cp in log:
         cp.wait_send()
-    for q in range(8):
-        keep = jnp.logical_and(inplace, 2 * q + odd == s.tp)
-
-        @pl.when(jnp.logical_not(keep))
-        def _():
-            landed(toks.at[pl.ds(16 * q, 16), own], x_s.at[q])
-
-    fans.drain()
+    turned_in(x_s)
+    landed(mo.at[:, pl.ds(0, 15 * LANES)], ring_s)
     turns.drain()
-    for g in gathers[0] + gathers[1]:
+    for g in gathers[0] + gathers[1] + fans:
         g.drain()
+    for q in sums[0] + sums[1]:
+        landed(xr.at[pl.ds(0, HALF), pl.ds(0, 15 * LANES)], q.ssem)
     landed(msg.at[pl.ds(0, 31)], d_s)
     landed(ret.at[pl.ds(0, 31)], r_s)
     landed(ent.at[pl.ds(0, 31)], e_s)
@@ -665,11 +610,6 @@
     V = pltpu.VMEM
     dma = pltpu.SemaphoreType.DMA
     S = jax.ShapeDtypeStruct
-    sums = lambda: [
-        V((4, HALF, LANES), BF), V((4, HALF, LANES), BF), V((4, CHUNK, LANES), BF), V((4, CHUNK, LANES), BF),
-        V((4, CHUNK, LANES), BF),
-        V((HALF, LANES), BF), V((HALF, LANES), BF), V((CHUNK, LANES), BF), V((CHUNK, LANES), BF),
-    ]
     operands = (x, cot, routes.T, rw.T, gate.T, ld.T, st.T, op, wg, wu, wd)
     gg, gu, gd, gop, ggb, gld, git = pl.pallas_call(
         body,
@@ -685,15 +625,15 @@
             V((32, MSG, LANES), BF), V((32, MSG, LANES), BF), V((ROWS, d), BF), V((ROWS, d), BF),
             V((d, 2 * LANES), BF), V((LANES, d), BF), V((ROWS, 2 * LANES), BF), V((ROWS, LANES), BF),
             V((4, 4, ROWS, LANES), BF), V((32, RET, LANES), BF), V((32, RET, LANES), BF),
-            *sums(), *sums(),
-            V(op.shape, BF), V((w, d), BF), V((w, d), BF), V((8, w, LANES), F32),
-            V((w, LANES), F32), V((w, LANES), F32), V((w, LANES), F32),
+            V((2, 2, 3, 4, HALF, LANES), BF), V((2, 2, 4, HALF, LANES), BF), V((2, 2, 3, HALF, LANES), BF),
+            V(op.shape, BF), V((w + w // 2, d), BF), V((w // 2, d), BF), V((8, w, LANES), F32),
+            V((w, LANES), F32), V((w, LANES), F32), V((w, LANES), F32), V((w, LANES), F32),
             V((LANES, d), BF), V((8, 2, 8, 16, LANES), BF), V((32, 1, w), F32), V((32, 1, w), F32),
             V((1, 1, w), F32), V((1, 1, w), F32), V((w, LANES), F32), V((w, LANES), F32),
-            dma((8,)), dma((3,)), dma, dma((2,)), dma((4,)), dma((4, 20)),
-            dma((2, 8)), dma((2, 8)), dma, dma((2,)),
-            dma, dma, dma((2, 2, 8)), dma((2, 2, 8)), dma((16,)), dma((16,)), dma((16,)), dma((16,)),
-            dma((8,)), dma((8,)), dma, dma, dma, dma, dma, dma, dma, dma, dma, dma,
+            dma((8,)), dma((3,)), dma, dma((2,)), dma((4,)), dma((4, 4)),
+            dma((2, 2)), dma((2, 2, 2)), dma, dma((2,)),
+            dma, dma, dma, dma((2, 8)), dma((2,)), dma((2, 4)), dma, dma,
+            dma, dma, dma, dma, dma, dma, dma, dma, dma, dma, dma, dma,
         ],
         compiler_params=pltpu.CompilerParams(
             collective_id=0, has_side_effects=True, vmem_limit_bytes=VMEM_MIB * 1024 * 1024

time: 102 us -> 92.7 us (0.909)
  Pallas kernels: 101 us -> 91.9 us
    pallas_call x1, Pallas kernels: 99.4 us -> 90.1 us  [step(): pl.pallas_call(body, out_shape=[S(wg.shape, F32), S(wu.shape, F32), S(wd....]
where the time goes in v3:
time: 92.7 us; the launch traced here: 92.5 us
  Pallas kernels  91.9 us (99%)
    pallas_call x1, Pallas kernels, step(): pl.pallas_call(body, out_shape=[S(wg.shape, F32), S(wu.shape, F32), S(wd....  90.1 us

profile of v3, /device:TPU:1, one launch (start us, length us, event | category | flops | bytes accessed | tf_op | source)
XLA Modules:
  0.0 92.5 jit_solution(825394423998027736)
XLA Ops:
  0.6 90.1 %whole_step.1 = (f32[1,2048,128]{2,1,0:T(8,128)S(1)}, f32[1,2048,128]{2,1,0:T(8,128)S(1)}, f32[1,128,2048]{2,1,0:T(8,128)S(1)}, f32[64,160]{1,0:T(8,128)S(1)}, b...) custom-call(bf16[128,128]{1,0:T(8,128)(2,1)} %x_in.1, bf16[128,128]{1,0:T(8,128)(2,1)} %cot_in.1, ...), custom_call_target="tpu_custom_call" | custom-call | tf_op jit(solution)/shard_map/whole_step/pallas_call | solution.py:614
  90.8 1.8 %settle.1 = (f32[1,2048,128]{2,1,0:T(8,128)}, f32[1,2048,128]{2,1,0:T(8,128)}, f32[1,128,2048]{2,1,0:T(8,128)}, f32[64,160]{1,0:T(8,128)}, bf16[160,128]{1,0:T(8...) custom-call(f32[1,2048,128]{2,1,0:T(8,128)S(1)} %get-tuple-element.21.refs_0_, ...), custom_call_target="tpu_custom_call" | custom-call | tf_op jit(solution)/shard_map/settle/pallas_call | solution.py:645

commit v4 on v3

--- a/solution.py
+++ b/solution.py
@@ -112,6 +112,46 @@
 
     def drain(self):
         landed(self.buf.at[self.rows, pl.ds(0, 15 * LANES)], self.ssem)
+
+
+class RelayGather(PlaneGather):
+    def fan(self, j):
+        view = self.view(self.fu[j], 0)
+        self.go(view, self.v, 1, 3 + 2 * j)
+        self.go(view, self.v, -1, 4 + 2 * j)
+
+    def stage0(self):
+        view = self.view(0, 0)
+        self.go(view, self.u, 1, 0)
+        self.go(view, self.u, -1, 1)
+
+    def pass_on(self, du, dv, axis, k, far):
+        for n, by in enumerate((1, -1)):
+            at = (-by, 0) if axis == self.u else (du, -by)
+            landed(self.view(*at), self.rsem.at[k + n])
+            self.go(self.view(*at, n), axis, by, far)
+            if axis == self.u:
+                self.fan(1 + n)
+
+    def stage1(self):
+        self.pass_on(0, 0, self.u, 0, 2)
+
+    def stage2(self):
+        landed(self.view(2, 0), self.rsem.at[2])
+        self.fan(3)
+
+    def stage3(self):
+        self.pass_on(0, 0, self.v, 3, 11)
+
+    def stage4(self):
+        self.pass_on(-1, 0, self.v, 5, 11)
+        self.pass_on(1, 0, self.v, 7, 11)
+
+    def stage5(self):
+        self.pass_on(2, 0, self.v, 9, 11)
+
+    def stage6(self):
+        landed(self.buf.at[self.rows, pl.ds(0, 4 * LANES)], self.rsem.at[11])
 
 
 class PlaneCast:
@@ -282,7 +322,7 @@
     barrier = pltpu.get_barrier_semaphore()
     peers = 1
     pl.semaphore_signal(barrier, inc=1, device_id=sibling, device_id_type=MESH)
-    for step in range(1, NZ):
+    for step in STEP_AT[:0:-1]:
         for core in range(2):
             pl.semaphore_signal(barrier, inc=1, device_id=dest(s, step, core), device_id_type=MESH)
             peers += 1
@@ -386,9 +426,6 @@
         lead = lead * jnp.where(iota(lead.shape, 1) >= 2**k, pltpu.roll(lead, 2**k, 1), 1.0)
     lead_v[...] = lead
     lastrow[0] = turned(states)[LANES - 1 :]
-    for chunk in range(2):
-        to_all(lambda k: whole.at[s.sp], lambda pos: whole.at[s.sp], w_s, w_r, dest, chunk)
-    send(lastrow, prevrow, l_s, l_r, (lax.rem(s.sp + 1, 32), s.tp), log)
 
     ri = iota((2 * CHUNK, 16 * MSG), 0)
     ci = iota((2 * CHUNK, 16 * MSG), 1)
@@ -425,7 +462,8 @@
         pair = []
         for n, (buf, u) in enumerate(((xr, "x"), (cr, "y"))):
             view = lane_blocks(buf, chunk * CHUNK, CHUNK)
-            pair.append(PlaneGather(s, view, u, g_s.at[2 * chunk + n], g_r.at[2 * chunk + n], buf, part))
+            kind = RelayGather if chunk == 0 else PlaneGather
+            pair.append(kind(s, view, u, g_s.at[2 * chunk + n], g_r.at[2 * chunk + n], buf, part))
         for g in pair:
             g.stage0()
         for g in pair:
@@ -471,25 +509,34 @@
 
     enter(0)
     gather(0, 1)
+    rung(0)
+    enter(1)
     gather(0, 2)
-    enter(1)
-    rung(0)
-    gather(1, 1)
     gather(0, 3)
     rung(1)
+    for chunk in range(2):
+        to_all(lambda k: whole.at[s.sp], lambda pos: whole.at[s.sp], w_s, w_r, dest, chunk)
+    send(lastrow, prevrow, l_s, l_r, (lax.rem(s.sp + 1, 32), s.tp), log)
+    gather(0, 4)
+    gather(1, 1)
+    rung(2)
+    gather(0, 5)
     gather(1, 2)
+    rung(3)
+    gather(0, 6)
+    rung(4)
     expert(0)
     gather(1, 3)
-    rung(2)
     expert(1)
+    rung(5)
     summed(0)
-    rung(3)
     summed(1)
+    rung(6)
     leave(0)
-    rung(4)
     leave(1)
+    rung(7)
+    send(mo.at[oprows, :], osib, h_s, h_r, sibling, log)
     back[pl.ds(s.c, 1)] = ret[pl.ds(s.c, 1)]
-    rung(5)
 
     @pl.loop(0, 8)
     def _(i):
@@ -499,7 +546,6 @@
         gu_out[0, lanes, :] = block[:, LANES:]
         gd_out[0, :, lanes] = dot_0(hid[...], cr[:, lanes])
 
-    rung(6)
     lane = iota((LANES, 32 * RET), 1)
     spots = down[:, 0:2].astype(I32)
     want = ((lane == spots[:, 0:1]) | (lane == spots[:, 1:2])).astype(F32).astype(BF)
@@ -541,8 +587,6 @@
         def _():
             landed(toks.at[pl.ds(0, 128), own], sem)
 
-    rung(7)
-    send(mo.at[oprows, :], osib, h_s, h_r, sibling, log)
     for k in (1, 2, 3):
         for f in fans:
             getattr(f, f"stage{k}")()
@@ -630,7 +674,7 @@
             V((w, LANES), F32), V((w, LANES), F32), V((w, LANES), F32), V((w, LANES), F32),
             V((LANES, d), BF), V((8, 2, 8, 16, LANES), BF), V((32, 1, w), F32), V((32, 1, w), F32),
             V((1, 1, w), F32), V((1, 1, w), F32), V((w, LANES), F32), V((w, LANES), F32),
-            dma((8,)), dma((3,)), dma, dma((2,)), dma((4,)), dma((4, 4)),
+            dma((8,)), dma((3,)), dma, dma((2,)), dma((4,)), dma((4, 12)),
             dma((2, 2)), dma((2, 2, 2)), dma, dma((2,)),
             dma, dma, dma, dma((2, 8)), dma((2,)), dma((2, 4)), dma, dma,
             dma, dma, dma, dma, dma, dma, dma, dma, dma, dma, dma, dma,

time: 92.7 us -> 92.1 us (level)
  no operation moved by 1% of the time
where the time goes in v4:
time: 92.1 us; the launch traced here: 92 us
  Pallas kernels  91.4 us (99%)
    pallas_call x1, Pallas kernels, step(): pl.pallas_call(body, out_shape=[S(wg.shape, F32), S(wu.shape, F32), S(wd....  89.6 us

profile of v4, /device:TPU:1, one launch (start us, length us, event | category | flops | bytes accessed | tf_op | source)
XLA Modules:
  0.0 92.0 jit_solution(13476843521210841564)
XLA Ops:
  0.6 89.6 %whole_step.1 = (f32[1,2048,128]{2,1,0:T(8,128)S(1)}, f32[1,2048,128]{2,1,0:T(8,128)S(1)}, f32[1,128,2048]{2,1,0:T(8,128)S(1)}, f32[64,160]{1,0:T(8,128)S(1)}, b...) custom-call(bf16[128,128]{1,0:T(8,128)(2,1)} %x_in.1, bf16[128,128]{1,0:T(8,128)(2,1)} %cot_in.1, ...), custom_call_target="tpu_custom_call" | custom-call | tf_op jit(solution)/shard_map/whole_step/pallas_call | solution.py:658
  90.2 1.8 %settle.1 = (f32[1,2048,128]{2,1,0:T(8,128)}, f32[1,2048,128]{2,1,0:T(8,128)}, f32[1,128,2048]{2,1,0:T(8,128)}, f32[64,160]{1,0:T(8,128)}, bf16[160,128]{1,0:T(8...) custom-call(f32[1,2048,128]{2,1,0:T(8,128)S(1)} %get-tuple-element.21.refs_0_, ...), custom_call_target="tpu_custom_call" | custom-call | tf_op jit(solution)/shard_map/settle/pallas_call | solution.py:689
